TPU v7x, 256 devices: a whole 4x4x8 slice. The times are simulated.
256 devices in a mesh: sp: 32 (over z, x), tp: 8 (over y, core).
Axes of the slice: x: 4, y: 4, z: 8, core: 2. Of those that a mesh axis runs over, the one named last changes fastest.
Arguments:
- residual: bfloat16 [16384, 2048], P('sp'), may hold values from -6 to 6
- queries: bfloat16 [16384, 1024], P('sp', 'tp'), may hold values from -384 to 384
- key_pairs: bfloat16 [16384, 1024], P('sp', 'tp'), may hold values from -384 to 384
- values: bfloat16 [16384, 1024], P('sp', 'tp'), may hold values from -6 to 6
- lambdas: float32 [8], P('tp'), may hold values from 0.3 to 0.8
- head_gain: float32 [128], replicated, may hold values from 0.1 to 1.9
- w_out: bfloat16 [1024, 2048], replicated, may hold values from -0.1875 to 0.1875
- norm_gain: float32 [2048], replicated, may hold values from 0.1 to 1.9
- w_gate: bfloat16 [2048, 5632], P('sp', 'tp'), may hold values from -0.125 to 0.125
- w_up: bfloat16 [2048, 5632], P('sp', 'tp'), may hold values from -0.125 to 0.125
- w_down: bfloat16 [5632, 2048], P('tp', 'sp'), may hold values from -0.078125 to 0.078125
Outputs:
- layer_out: bfloat16 [16384, 2048], P(('sp', 'tp'))
All inputs are finite; a program needn't handle non-finite values.
Results may differ from a plain program's by a relative error of at most 0.018.
Values may be sent and summed in bfloat16 or wider, within the bound.
A program may use at most 128 MiB of HBM per device.

v0:
```python
import math

import jax
import jax.numpy as jnp
from jax import lax
from jax.sharding import Mesh
from jax.sharding import PartitionSpec as P

HD = 64
SP = ("sp_0", "sp_1")
SP_TP = ("sp_0", "sp_1", "tp")


def sent_together(arrays, axis, dim, along):
    both = jnp.concatenate(arrays, axis=along)
    result, at, finished = (lax.all_gather(both, axis, axis=dim, tiled=True), 0, [])
    for a in arrays:
        finished.append(lax.slice_in_dim(result, at, at + a.shape[along], axis=along))
        at += a.shape[along]
    return tuple(finished)


def copy_for_each(shard, axis):
    length = lax.axis_size(axis)
    return lax.all_to_all(
        jnp.broadcast_to(shard[None], (length, *shard.shape)), axis, 0, 0, tiled=True
    )


def laid_out(parts, dim):
    parts = jnp.moveaxis(parts, 0, dim)
    dims = parts.shape
    return parts.reshape(*dims[:dim], dims[dim] * dims[dim + 1], *dims[dim + 2 :])


def gather_directly(shard, axis, dim):
    parts = copy_for_each(shard, axis)
    return laid_out(parts, dim)


def whole_of(shard, axes, dim):
    result = shard
    for number in range(len(axes) - 1, -1, -1):
        result = lax.all_gather(result, axes[number], axis=dim, tiled=True)
    return result


def in_blocks(shard, dim, length):
    before, after = (shard.shape[:dim], shard.shape[dim + 1 :])
    return jnp.moveaxis(shard.reshape(*before, length, -1, *after), dim, 0)


def summed_on_arrival(shard, axis, dim):
    parts = in_blocks(shard, dim, lax.axis_size(axis))
    arrived = lax.all_to_all(parts, axis, split_axis=0, concat_axis=0, tiled=True)
    return arrived.astype(jnp.float32).sum(axis=0)


def per_device(
    residual, queries, key_pairs, values, lambdas, head_gain, w_out, norm_gain, w_gate, w_up, w_down
):
    local_rows = queries.shape[0]
    heads_here = lambdas.shape[0]
    value_width = values.shape[1] // heads_here
    score_scale = HD ** (-0.5)
    query_view = queries.reshape(local_rows, heads_here, 2, HD)

    def update(carry, key_block, value_block):
        highest, totals, mixture = carry
        scores = (
            jnp.einsum("qhmd,khmd->hmqk", query_view, key_block, preferred_element_type=jnp.float32)
            * score_scale
        )
        new_high = jnp.maximum(highest, jnp.max(scores, axis=-1))
        shrink = jnp.exp(highest - new_high)
        weights = jnp.exp(scores - new_high[..., None])
        totals = totals * shrink + jnp.sum(weights, axis=-1)
        mixture = mixture * shrink[..., None] + jnp.einsum(
            "hmqk,khe->hmqe",
            weights.astype(jnp.bfloat16),
            value_block,
            preferred_element_type=jnp.float32,
        )
        return (new_high, totals, mixture)

    initial = (
        jnp.full((heads_here, 2, local_rows), -jnp.inf, jnp.float32),
        jnp.zeros((heads_here, 2, local_rows), jnp.float32),
        jnp.zeros((heads_here, 2, local_rows, value_width), jnp.float32),
    )
    key_piece, value_piece = sent_together((key_pairs, values), SP, 0, 1)
    length = key_piece.shape[0]
    span = math.gcd(length, 512)
    key_blocks = key_piece.reshape(length // span, span, heads_here, 2, HD)
    value_blocks = value_piece.reshape(length // span, span, heads_here, value_width)

    def advance(position, inner):
        return update(inner, key_blocks[position], value_blocks[position])

    highest, totals, mixture = lax.fori_loop(0, length // span, advance, initial)
    mixed = mixture / totals[..., None]
    differ = mixed[:, 0] - lambdas[:, None, None] * mixed[:, 1]
    normed_heads = (
        differ * lax.rsqrt(jnp.mean(differ * differ, axis=-1, keepdims=True) + 1e-05) * head_gain
    )
    heads_out = (
        jnp.transpose(normed_heads, (1, 0, 2))
        .reshape(local_rows, heads_here * value_width)
        .astype(jnp.bfloat16)
    )
    tp_index = lax.axis_index("tp")
    own_rows = local_rows // lax.axis_size("tp")
    own_begin = tp_index * own_rows
    token_heads = lax.all_to_all(heads_out, "tp", split_axis=0, concat_axis=1, tiled=True)
    projected = jnp.dot(token_heads, w_out, preferred_element_type=jnp.float32)
    residual_own = lax.dynamic_slice_in_dim(residual, own_begin, own_rows, 0)
    hidden_own = (residual_own.astype(jnp.float32) + projected).astype(jnp.bfloat16)
    stream_f = hidden_own.astype(jnp.float32)
    scaled = stream_f * lax.rsqrt(jnp.mean(stream_f * stream_f, axis=-1, keepdims=True) + 1e-05)
    normed_rows = gather_directly((scaled * norm_gain).astype(jnp.bfloat16), "tp", 0)
    unit_width = w_gate.shape[1]
    joined = jnp.concatenate([w_gate, w_up], axis=1)
    both_sums = jnp.dot(normed_rows, whole_of(joined, SP, 0), preferred_element_type=jnp.float32)
    gate_sum = both_sums[:, :unit_width]
    up_sum = both_sums[:, unit_width:]
    hidden_units = (jax.nn.silu(gate_sum) * up_sum).astype(jnp.bfloat16)
    down_whole = whole_of(w_down, SP, 1)
    ffn_out = summed_on_arrival(
        jnp.dot(hidden_units, down_whole, preferred_element_type=jnp.float32).astype(jnp.bfloat16),
        "tp",
        0,
    )
    return (hidden_own.astype(jnp.float32) + ffn_out).astype(jnp.bfloat16)


def solution(mesh):
    torus = Mesh(mesh.devices.reshape(8, 4, mesh.shape["tp"]), ("sp_0", "sp_1", "tp"))
    return jax.shard_map(
        per_device,
        mesh=torus,
        in_specs=(
            P(SP, None),
            P(SP, "tp"),
            P(SP, "tp"),
            P(SP, "tp"),
            P("tp"),
            P(),
            P(),
            P(),
            P(SP, "tp"),
            P(SP, "tp"),
            P("tp", SP),
        ),
        out_specs=P(SP_TP, None),
        check_vma=False,
    )
```

profile of v0, /device:TPU:1, one launch (start us, length us, event | category | flops | bytes accessed | tf_op | source)
XLA Modules:
  0.0 355.4 jit_solution(6053489746740450555)
XLA Ops:
  6.5 1.7 pad_maximum_fusion
  9.4 13.2 %all_gather.16 = bf16[256,1408]{1,0:T(8,128)(2,1)} all-gather(bf16[64,1408]{1,0:T(8,128)(2,1)S(1)} %pad_maximum_fusion.1), channel_id=1, replica_groups=mesh['sp_0'=8,'sp_1'=4,'tp'=8] {'sp_1'}, dimensions={0}, use_global_device_ids=true | all-gather | bytes 901120 | tf_op jit(solution)/shard_map/all_gather | solution.py:44
  22.7 11.4 %all_gather.18 = bf16[704,256]{0,1:T(8,128)(2,1)} all-gather(bf16[704,64]{0,1:T(8,128)(2,1)S(1)} %copy-done.1), channel_id=1, replica_groups=mesh['sp_0'=8,'sp_1'=4,'tp'=8] {'sp_1'}, dimensions={1}, use_global_device_ids=true | all-gather | bytes 450560 | tf_op jit(solution)/shard_map/all_gather | solution.py:44
  34.9 75.9 %all-gather.4.cloned.1.call-done = bf16[16384,256]{1,0:T(8,128)(2,1)} async-done(((bf16[512,256]{1,0:T(8,128)(2,1)}), bf16[16384,256]{1,0:T(8,128)(2,1)}) %all-gather.4.cloned.1.call-update) | async-done | bytes 8388624 | tf_op jit(solution)/shard_map/all_gather | solution.py:16
  110.9 5.7 %fusion.27 = (bf16[16384,128]{1,0:T(8,128)(2,1)}, bf16[16384,128]{1,0:T(8,128)(2,1)}) fusion(bf16[16384,256]{1,0:T(8,128)(2,1)} %all-gather.4.cloned.1.call-done), kind=kLoop, calls=%fused_computation.48 | loop fusion | bytes 16777216 | tf_op jit(solution)/shard_map/slice | solution.py:18
  116.6 14.8 %reshape.168 = bf16[32,512,1,2,64]{4,3,1,0,2:T(2,128)(2,1)} reshape(bf16[16384,128]{1,0:T(8,128)(2,1)} %get-tuple-element.198) | data formatting | bytes 8388608 | tf_op jit(solution)/shard_map/reshape | solution.py:94
  131.4 18.4 %copy.28 = bf16[32,512,1,2,64]{1,4,3,2,0:T(8,128)(2,1)} copy(bf16[32,512,1,2,64]{4,3,1,0,2:T(2,128)(2,1)} %reshape.168) | data formatting | bytes 8388608
  149.8 108.3 %while.18 = (s32[]{:T(128)}, f32[1,2,512]{2,1,0:T(2,128)S(1)}, f32[1,2,512]{2,1,0:T(2,128)S(1)}, f32[1,2,512,128]{3,2,1,0:T(8,128)S(1)}, bf16[32,512,1,2,64]{1,4...) while((s32[]{:T(128)}, f32[1,2,512]{2,1,0:T(2,128)S(1)}, ...), condition=%wide.region_3.0_spmd.clone, body=%wide.region_0.0_spmd.clone.sunk | while | flops 205920256 | bytes 7799913 | solution.py:100
  151.2 1.5 fusion.43
  154.6 1.5 fusion.43
  161.4 1.5 fusion.43
  164.8 1.5 fusion.43
  168.1 1.5 fusion.43
  185.1 1.5 fusion.43
  188.5 1.5 fusion.43
  195.2 1.5 fusion.43
  202.0 1.5 fusion.43
  205.4 1.5 fusion.43
  212.2 1.5 fusion.43
  215.5 1.5 fusion.43
  218.9 1.5 fusion.43
  232.5 1.5 fusion.43
  252.8 1.5 fusion.43
  259.4 5.7 %all-to-all-start = ((bf16[8,64,128]{2,1,0:T(8,128)(2,1)}), bf16[8,64,128]{2,1,0:T(8,128)(2,1)S(1)}, u32[]{:S(2)}, u32[]{:S(2)}) async-start(bf16[8,64,128]{2,1,0:T(8,128)(2,1)} %multiply_convert_fusion.1), calls=%async_computation | async-start | bytes 262144 | tf_op jit(solution)/shard_map/all_to_all | solution.py:114
  265.1 5.2 %all-to-all-done = bf16[8,64,128]{2,1,0:T(8,128)(2,1)S(1)} async-done(((bf16[8,64,128]{2,1,0:T(8,128)(2,1)}), bf16[8,64,128]{2,1,0:T(8,128)(2,1)S(1)}, u32[]{:S(2)}, u32[]{:S(2)}) %all-to-all-start) | async-done | bytes 131104 | tf_op jit(solution)/shard_map/all_to_all | solution.py:114
  270.3 3.2 multiply_reduce_fusion
  273.6 1.6 broadcast_in_dim.30
  275.2 4.4 %all-to-all-start.1 = ((bf16[8,64,2048]{2,1,0:T(8,128)(2,1)}), bf16[8,64,2048]{2,1,0:T(8,128)(2,1)S(1)}, u32[]{:S(2)}, u32[]{:S(2)}) async-start(bf16[8,64,2048]{2,1,0:T(8,128)(2,1)} %broadcast_in_dim.30), calls=%async_computation.1 | async-start | bytes 4194304 | tf_op jit(solution)/shard_map/all_to_all | solution.py:25
  279.6 26.2 %all-to-all-done.1 = bf16[8,64,2048]{2,1,0:T(8,128)(2,1)S(1)} async-done(((bf16[8,64,2048]{2,1,0:T(8,128)(2,1)}), bf16[8,64,2048]{2,1,0:T(8,128)(2,1)S(1)}, u32[]{:S(2)}, u32[]{:S(2)}) %all-to-all-start.1) | async-done | bytes 2097184 | tf_op jit(solution)/shard_map/all_to_all | solution.py:25
  305.8 7.6 %fusion.28 = f32[512,1408]{1,0:T(8,128)} fusion(bf16[512,2048]{1,0:T(8,128)(2,1)S(1)} %bitcast.83, bf16[2048,1408]{1,0:T(8,128)(2,1)} %all-gather.6.cloned.1.call-done), kind=kOutput, calls=%fused_computation.49 | convolution fusion | flops 2952790016 | bytes 10747904 | tf_op jit(solution)/shard_map/dot_general | solution.py:123
  313.5 4.7 %convolution_convert_fusion = bf16[512,2048]{1,0:T(8,128)(2,1)S(1)} fusion(bf16[704,2048]{0,1:T(8,128)(2,1)} %all-gather.8.cloned.1.call-done, f32[512,1408]{1,0:T(8,128)} %fusion.28), kind=kOutput, calls=%fused_computation.26 | convolution fusion | flops 1479606272 | bytes 8388608 | tf_op jit(solution)/shard_map/dot_general | solution.py:129
  318.2 29.6 %all_to_all.26 = bf16[8,64,2048]{2,1,0:T(8,128)(2,1)S(1)} all-to-all(bf16[8,64,2048]{2,1,0:T(8,128)(2,1)S(1)} %bitcast.84), channel_id=1, replica_groups=mesh['sp_0'=8,'sp_1'=4,'tp'=8] {'tp'}, dimensions={0} | all-to-all | bytes 4194304 | tf_op jit(solution)/shard_map/all_to_all | solution.py:55
  (207 shorter events, 87.6 us)
Async XLA Ops:
  6.5 16.2 %copy-start.1 = (bf16[704,64]{0,1:T(8,128)(2,1)S(1)}, bf16[704,64]{0,1:T(8,128)(2,1)}, u32[]{:S(2)}) copy-start(bf16[704,64]{0,1:T(8,128)(2,1)} %param.23) | copy-start | bytes 270340
  6.5 27.6 %copy-start = (bf16[512,128]{1,0:T(8,128)(2,1)S(1)}, bf16[512,128]{1,0:T(8,128)(2,1)}, u32[]{:S(2)}) copy-start(bf16[512,128]{1,0:T(8,128)(2,1)} %param.14) | copy-start | bytes 393220
  6.5 104.4 %all-gather.4.cloned.1.call-start = ((), (), s32[]{:S(2)}) async-start(), calls=%async_computation.3 | async-start | bytes 8650752 | tf_op jit(solution)/shard_map/all_gather | solution.py:16
  8.3 271.3 %all-gather.6.cloned.1.call-start = ((), (), s32[]{:S(2)}) async-start(), calls=%async_computation.4 | async-start | bytes 6488064 | tf_op jit(solution)/shard_map/all_gather | solution.py:44
  22.6 290.8 %all-gather.8.cloned.1.call-start = ((), (), s32[]{:S(2)}) async-start(), calls=%async_computation.5 | async-start | bytes 3538944 | tf_op jit(solution)/shard_map/all_gather | solution.py:44
  149.8 108.8 %copy-start.3 = (f32[128]{0:T(128)S(1)}, f32[128]{0:T(128)}, u32[]{:S(2)}) copy-start(f32[128]{0:T(128)} %param.18) | copy-start | bytes 1540
  259.4 10.9 %all-to-all-start = ((bf16[8,64,128]{2,1,0:T(8,128)(2,1)}), bf16[8,64,128]{2,1,0:T(8,128)(2,1)S(1)}, u32[]{:S(2)}, u32[]{:S(2)}) async-start(bf16[8,64,128]{2,1,0:T(8,128)(2,1)} %multiply_convert_fusion.1), calls=%async_computation | async-start | bytes 262144 | tf_op jit(solution)/shard_map/all_to_all | solution.py:114
  265.1 8.4 %copy-start.2 = (f32[2048]{0:T(1024)S(1)}, f32[2048]{0:T(1024)}, u32[]{:S(2)}) copy-start(f32[2048]{0:T(1024)} %param.20) | copy-start | bytes 24580
  275.2 30.6 %all-to-all-start.1 = ((bf16[8,64,2048]{2,1,0:T(8,128)(2,1)}), bf16[8,64,2048]{2,1,0:T(8,128)(2,1)S(1)}, u32[]{:S(2)}, u32[]{:S(2)}) async-start(bf16[8,64,2048]{2,1,0:T(8,128)(2,1)} %broadcast_in_dim.30), calls=%async_computation.1 | async-start | bytes 4194304 | tf_op jit(solution)/shard_map/all_to_all | solution.py:25
Sparse Core Ops, SparseCore 0:
  9.9 100.9 all-gather.3
  112.7 67.1 all-gather.5
  181.7 43.1 all-gather.7
where the time goes:
time: 358 us; the launch traced here: 355 us
  matrix products  110 us (31%)
  waiting for transfers between devices  107 us (30%)
  blocking collectives  54.2 us (15%)
  local copies, waits for them, and re-layouts  40.7 us (11%)
  other arithmetic  17.9 us (5%)
  between operations  13.9 us (4%)
  starting transfers between devices  10.2 us (3%)
    all_gather x1, waiting for transfers between devices, sent_together(): lax.all_gather(both, axis, axis=dim, tiled=True)  75.9 us
    dot_general x32, matrix products, update(): jnp.einsum('hmqk,khe->hmqe', weights.astype(jnp.bfloat16), value_block, p...  49.2 us
    dot_general x32, matrix products, update(): jnp.einsum('qhmd,khmd->hmqk', query_view, key_block, preferred_element_ty...  44.9 us
    all_to_all x1, blocking collectives, summed_on_arrival(): lax.all_to_all(parts, axis, split_axis=0, concat_axis=0, tiled=True)  29.6 us
    all_to_all x1, waiting for transfers between devices, copy_for_each(): lax.all_to_all(jnp.broadcast_to(shard[None], (length, *shard.shape)), axi...  26.2 us
    all_gather x2, blocking collectives, whole_of(): result = lax.all_gather(result, axes[number], axis=dim, tiled=True)  24.6 us
    unnamed x10, local copies, waits for them, and re-layouts  18.5 us
    reshape x1, local copies, waits for them, and re-layouts, per_device(): key_blocks = key_piece.reshape(length // span, span, heads_here, 2, HD)  14.8 us
  transfers between devices with their start and end apart: 5, of which 3 were waited for; matrix products, arithmetic and copies ran while one was open for 45% of the time, Pallas kernels for 0%

commit v1 on v0

v1 whole, which is shorter than its diff:
```python
import functools

import jax
import jax.numpy as jnp
from jax import lax
from jax.experimental import pallas as pl
from jax.experimental.pallas import tpu as pltpu
from jax.sharding import Mesh
from jax.sharding import PartitionSpec as P

HD = 64
SP = ("sp_0", "sp_1")
SP_TP = ("sp_0", "sp_1", "tp")
LOWEST = -1e30
EXTRA = 16


def spread_queries(q, out_ref, at):
    rows = q.shape[0]
    lane = lax.broadcasted_iota(jnp.int32, q.shape, 1)
    zero = jnp.zeros_like(q)
    out_ref[pl.ds(at, rows), :] = jnp.where(lane < HD, q, zero)
    out_ref[pl.ds(at + rows, rows), :] = jnp.where(lane >= HD, q, zero)


def attend_tile(q2, keys, values_t, high_ref, acc_ref):
    scores = lax.dot_general(
        keys, q2, (((1,), (1,)), ((), ())), preferred_element_type=jnp.float32
    )
    before = high_ref[...]
    after = jnp.maximum(before, jnp.max(scores, axis=0, keepdims=True))
    shrink = jnp.exp(before - after)
    weights = jnp.exp(scores - after).astype(jnp.bfloat16)
    mixed = jnp.dot(values_t, weights, preferred_element_type=jnp.float32)
    acc_ref[...] = acc_ref[...] * shrink + mixed
    high_ref[...] = after


def attention_kernel(q_ref, k_ref, vt_ref, o_ref, lse_ref, q2, high, acc):
    groups, rows, _ = q_ref.shape
    width = vt_ref.shape[1] - EXTRA
    for g in range(groups):
        spread_queries(q_ref[g], q2, g * 2 * rows)
    high[...] = jnp.full_like(high, LOWEST)
    acc[...] = jnp.zeros_like(acc)

    def step(i, c):
        attend_tile(q2[...], k_ref[i], vt_ref[i], high, acc)
        return c

    lax.fori_loop(0, k_ref.shape[0], step, 0)
    for g in range(groups):
        cols = pl.ds(g * 2 * rows, 2 * rows)
        totals = acc[pl.ds(width, 1), cols]
        o_ref[g] = (acc[pl.ds(0, width), cols] / totals).astype(o_ref.dtype)
        lse_ref[g] = jnp.broadcast_to(high[:, cols] + jnp.log(totals), (8, 2 * rows))


def attention(q_all, k_all, vt_all):
    groups, rows, _ = q_all.shape
    width = vt_all.shape[1] - EXTRA
    columns = groups * 2 * rows
    return pl.pallas_call(
        attention_kernel,
        out_shape=(
            jax.ShapeDtypeStruct((groups, width, 2 * rows), jnp.bfloat16),
            jax.ShapeDtypeStruct((groups, 8, 2 * rows), jnp.float32),
        ),
        in_specs=[pl.BlockSpec(memory_space=pltpu.VMEM)] * 3,
        out_specs=[pl.BlockSpec(memory_space=pltpu.VMEM)] * 2,
        scratch_shapes=[
            pltpu.VMEM((columns, 2 * HD), jnp.bfloat16),
            pltpu.VMEM((1, columns), jnp.float32),
            pltpu.VMEM((width + EXTRA, columns), jnp.float32),
        ],
        cost_estimate=pl.CostEstimate(
            flops=30_000_000_000, bytes_accessed=8_000_000, transcendentals=16_000_000
        ),
        compiler_params=pltpu.CompilerParams(vmem_limit_bytes=56 * 2**20),
    )(q_all, k_all, vt_all)


def laid_out(parts, dim):
    parts = jnp.moveaxis(parts, 0, dim)
    dims = parts.shape
    return parts.reshape(*dims[:dim], dims[dim] * dims[dim + 1], *dims[dim + 2 :])


def gather_directly(shard, axis, dim):
    length = lax.axis_size(axis)
    parts = lax.all_to_all(
        jnp.broadcast_to(shard[None], (length, *shard.shape)), axis, 0, 0, tiled=True
    )
    return laid_out(parts, dim)


def summed_on_arrival(shard, axis):
    length = lax.axis_size(axis)
    parts = shard.reshape(length, shard.shape[0] // length, shard.shape[1])
    arrived = lax.all_to_all(parts, axis, split_axis=0, concat_axis=0, tiled=True)
    return arrived.astype(jnp.float32).sum(axis=0)


def per_device(
    residual, queries, key_pairs, values, lambdas, head_gain, w_out, norm_gain, w_gate, w_up, w_down
):
    local_rows = queries.shape[0]
    scaled_q = queries * jnp.bfloat16(HD**-0.5)
    k_all = lax.all_gather(key_pairs, "sp_0", axis=0)
    extra = jnp.concatenate(
        [jnp.ones((1, local_rows), jnp.bfloat16), jnp.zeros((EXTRA - 1, local_rows), jnp.bfloat16)]
    )
    vt = lax.all_gather(values.T, "sp_0", axis=0)
    vt_all = jnp.concatenate([vt, jnp.broadcast_to(extra, (vt.shape[0], *extra.shape))], axis=1)
    q_all = lax.all_gather(scaled_q, "sp_1", axis=0)
    mixed_part, lse_part = attention(q_all, k_all, vt_all)
    mixed_part = lax.all_to_all(mixed_part, "sp_1", 0, 0, tiled=True).astype(jnp.float32)
    lse_part = lax.all_to_all(lse_part, "sp_1", 0, 0, tiled=True)[:, :1]
    share = jnp.exp(lse_part - jnp.max(lse_part, axis=0, keepdims=True))
    share = share / jnp.sum(share, axis=0, keepdims=True)
    mixed = jnp.sum(mixed_part * share, axis=0)
    differ = mixed[:, :local_rows] - lambdas[0] * mixed[:, local_rows:]
    normed_heads = (
        differ
        * lax.rsqrt(jnp.mean(differ * differ, axis=0, keepdims=True) + 1e-05)
        * head_gain[:, None]
    )
    heads_out = normed_heads.T.astype(jnp.bfloat16)
    tp_index = lax.axis_index("tp")
    own_rows = local_rows // lax.axis_size("tp")
    own_begin = tp_index * own_rows
    token_heads = lax.all_to_all(heads_out, "tp", split_axis=0, concat_axis=1, tiled=True)
    projected = jnp.dot(token_heads, w_out, preferred_element_type=jnp.float32)
    residual_own = lax.dynamic_slice_in_dim(residual, own_begin, own_rows, 0)
    hidden_own = (residual_own.astype(jnp.float32) + projected).astype(jnp.bfloat16)
    stream_f = hidden_own.astype(jnp.float32)
    scaled = stream_f * lax.rsqrt(jnp.mean(stream_f * stream_f, axis=-1, keepdims=True) + 1e-05)
    normed_rows = gather_directly((scaled * norm_gain).astype(jnp.bfloat16), "tp", 0)
    unit_width = w_gate.shape[1]
    joined = jnp.concatenate([w_gate, w_up], axis=1)
    w_all = lax.all_gather(joined, SP, axis=0, tiled=True)
    both_sums = jnp.dot(normed_rows, w_all, preferred_element_type=jnp.float32)
    gate_sum = both_sums[:, :unit_width]
    up_sum = both_sums[:, unit_width:]
    hidden_units = (jax.nn.silu(gate_sum) * up_sum).astype(jnp.bfloat16)
    down_t = lax.all_gather(w_down.T, SP, axis=0, tiled=True)
    ffn_part = lax.dot_general(
        hidden_units, down_t, (((1,), (1,)), ((), ())), preferred_element_type=jnp.float32
    )
    ffn_out = summed_on_arrival(ffn_part.astype(jnp.bfloat16), "tp")
    return (hidden_own.astype(jnp.float32) + ffn_out).astype(jnp.bfloat16)


def solution(mesh):
    torus = Mesh(mesh.devices.reshape(8, 4, mesh.shape["tp"]), ("sp_0", "sp_1", "tp"))
    return jax.shard_map(
        per_device,
        mesh=torus,
        in_specs=(
            P(SP, None),
            P(SP, "tp"),
            P(SP, "tp"),
            P(SP, "tp"),
            P("tp"),
            P(),
            P(),
            P(),
            P(SP, "tp"),
            P(SP, "tp"),
            P("tp", SP),
        ),
        out_specs=P(SP_TP, None),
        check_vma=False,
    )
```

time: 358 us -> 301 us (0.84)
  matrix products: 110 us -> 15.6 us
  local copies, waits for them, and re-layouts: 40.7 us -> 2.51 us
  blocking collectives: 54.2 us -> 85.9 us
  waiting for transfers between devices: 107 us -> 135 us
  Pallas kernels: 0 us -> 26.4 us
  other arithmetic: 17.9 us -> 5.48 us
  starting transfers between devices: 10.2 us -> 16.2 us
    dot_general x66 -> x2, matrix products: 106 us -> 12.3 us  [the longest x1 7.65 us: per_device(): both_sums = jnp.dot(normed_rows, w_all, preferred_element_type=jnp.float32)]
    all_gather x3 -> x4, waiting for transfers between devices: 76 us -> 119 us  [the longest x1 59.1 us: per_device(): down_t = lax.all_gather(w_down.T, SP, axis=0, tiled=True)]
    all_to_all x0 -> x2, blocking collectives: none -> 38.3 us  [the longest x1 29.4 us: gather_directly(): lax.all_to_all(jnp.broadcast_to(shard[None], (length, *shard.shape)), axi...]
    pallas_call x0 -> x1, Pallas kernels: none -> 26.4 us  [attention(): pl.pallas_call(attention_kernel, out_shape=(jax.ShapeDtypeStruct((groups,...]
    unnamed x10 -> x7, local copies, waits for them, and re-layouts: 18.5 us -> 0.02 us
    all_to_all x1, waiting for transfers between devices: 26.2 us -> 8.93 us  [per_device(): lax.all_to_all(mixed_part, 'sp_1', 0, 0, tiled=True).astype(jnp.float32)]
    reshape x1 -> x0, local copies, waits for them, and re-layouts: 14.8 us -> none  [per_device(): key_blocks = key_piece.reshape(length // span, span, heads_here, 2, HD)]
    all_gather x2 -> x1, blocking collectives: 24.6 us -> 12.8 us  [per_device(): q_all = lax.all_gather(scaled_q, 'sp_1', axis=0)]
  transfers between devices with their start and end apart: 5 -> 6, of which waited for: 3 -> 5; matrix products, arithmetic and copies ran while one was open for 45% -> 6% of each run, Pallas kernels for 0% -> 9%
where the time goes in v1:
time: 301 us
  waiting for transfers between devices  135 us (45%)
  blocking collectives  85.9 us (29%)
  Pallas kernels  26.4 us (9%)
  starting transfers between devices  16.2 us (5%)
  matrix products  15.6 us (5%)
  between operations  13.9 us (5%)
  other arithmetic  5.48 us (2%)
    all_gather x1, waiting for transfers between devices, per_device(): down_t = lax.all_gather(w_down.T, SP, axis=0, tiled=True)  59.1 us
    all_gather x1, waiting for transfers between devices, per_device(): k_all = lax.all_gather(key_pairs, 'sp_0', axis=0)  36.6 us
    all_to_all x1, blocking collectives, summed_on_arrival(): lax.all_to_all(parts, axis, split_axis=0, concat_axis=0, tiled=True)  34.8 us
    all_to_all x1, blocking collectives, gather_directly(): lax.all_to_all(jnp.broadcast_to(shard[None], (length, *shard.shape)), axi...  29.4 us
    pallas_call x1, Pallas kernels, attention(): pl.pallas_call(attention_kernel, out_shape=(jax.ShapeDtypeStruct((groups,...  26.4 us
    all_gather x1, waiting for transfers between devices, per_device(): vt = lax.all_gather(values.T, 'sp_0', axis=0)  23.1 us
    all_gather x1, blocking collectives, per_device(): q_all = lax.all_gather(scaled_q, 'sp_1', axis=0)  12.8 us
    all_to_all x1, starting transfers between devices, per_device(): lax.all_to_all(heads_out, 'tp', split_axis=0, concat_axis=1, tiled=True)  12.5 us
  transfers between devices with their start and end apart: 6, of which 5 were waited for; matrix products, arithmetic and copies ran while one was open for 6% of the time, Pallas kernels for 9%

profile of v1, /device:TPU:1, one launch (start us, length us, event | category | flops | bytes accessed | tf_op | source)
XLA Modules:
  0.0 300.9 jit_solution(4797118897078790608)
XLA Ops:
  6.5 0.7 all-gather.14.cloned.1.call-update
  7.3 0.7 all-gather.12.cloned.1.call-update
  8.0 0.0 all-gather.8.cloned.1.call-start
  8.1 1.7 pad_maximum_fusion.1
  9.8 0.0 all-gather.10.cloned.1.call-start
  9.8 0.5 all-gather.10.cloned.1.call-update
  10.4 0.9 broadcast_multiply_fusion
  11.3 12.8 %all-gather = bf16[2048,128]{1,0:T(8,128)(2,1)} all-gather(bf16[512,128]{1,0:T(8,128)(2,1)S(1)} %broadcast_multiply_fusion), channel_id=2, replica_groups=mesh['sp_0'=8,'sp_1'=4,'tp'=8] {'sp_1'}, dimensions={0}, use_global_device_ids=true | all-gather | bytes 655360 | tf_op jit(solution)/shard_map/all_gather | solution.py:115
  24.1 23.1 %all-gather.14.cloned.1.call-done = bf16[1024,512]{0,1:T(8,128)(2,1)} async-done(((bf16[128,512]{0,1:T(8,128)(2,1)}), bf16[1024,512]{0,1:T(8,128)(2,1)}) %all-gather.14.cloned.1.call-update) | async-done | bytes 1048592 | tf_op jit(solution)/shard_map/all_gather | solution.py:113
  47.1 1.5 copy.15
  48.7 1.1 pad_maximum_fusion.vt_ref
  49.8 36.6 %all-gather.12.cloned.1.call-done = bf16[4096,128]{1,0:T(8,128)(2,1)} async-done(((bf16[512,128]{1,0:T(8,128)(2,1)}), bf16[4096,128]{1,0:T(8,128)(2,1)}) %all-gather.12.cloned.1.call-update) | async-done | bytes 1048592 | tf_op jit(solution)/shard_map/all_gather | solution.py:109
  86.4 26.4 %shard_map.109 = (bf16[4,128,1024]{2,1,0:T(8,128)(2,1)}, f32[4,8,1024]{2,1,0:T(8,128)}) custom-call(bf16[4,512,128]{2,1,0:T(8,128)(2,1)} %bitcast.33, bf16[8,512,128]{2,1,0:T(8,128)(2,1)} %bitcast.37, bf16[8,144,512]{2,1,0:T(8,128)(2,1)} %pad_maximum_fusion.vt_ref), custom_call_target="tpu_custom_call" | custom-call | flops 30000001024 | bytes 8000000 | tf_op jit(solution)/shard_map/pallas_call | solution.py:63
  112.8 8.9 %all_to_all.39 = f32[4,8,1024]{2,1,0:T(8,128)S(1)} all-to-all(f32[4,8,1024]{2,1,0:T(8,128)} %get-tuple-element.8), channel_id=1, replica_groups=mesh['sp_0'=8,'sp_1'=4,'tp'=8] {'sp_1'}, dimensions={0} | all-to-all | bytes 262144 | tf_op jit(solution)/shard_map/all_to_all | solution.py:118
  121.7 3.6 %all-to-all-start = ((bf16[4,128,1024]{2,1,0:T(8,128)(2,1)}), bf16[4,128,1024]{2,1,0:T(8,128)(2,1)S(1)}, u32[]{:S(2)}, u32[]{:S(2)}) async-start(bf16[4,128,1024]{2,1,0:T(8,128)(2,1)} %get-tuple-element.7), calls=%async_computation | async-start | bytes 2097152 | tf_op jit(solution)/shard_map/all_to_all | solution.py:117
  126.1 8.9 %all-to-all-done = bf16[4,128,1024]{2,1,0:T(8,128)(2,1)S(1)} async-done(((bf16[4,128,1024]{2,1,0:T(8,128)(2,1)}), bf16[4,128,1024]{2,1,0:T(8,128)(2,1)S(1)}, u32[]{:S(2)}, u32[]{:S(2)}) %all-to-all-start) | async-done | bytes 1048608 | tf_op jit(solution)/shard_map/all_to_all | solution.py:117
  135.0 0.2 multiply_reduce_fusion
  135.2 0.1 multiply_reduce_fusion.2
  135.3 0.1 fusion.6
  135.4 0.8 copy.16
  136.2 12.5 %all-to-all-start.2 = ((bf16[8,64,128]{2,1,0:T(8,128)(2,1)}), bf16[8,64,128]{2,1,0:T(8,128)(2,1)S(1)}, u32[]{:S(2)}, u32[]{:S(2)}) async-start(bf16[8,64,128]{2,1,0:T(8,128)(2,1)} %bitcast.6), calls=%async_computation.2 | async-start | bytes 262144 | tf_op jit(solution)/shard_map/all_to_all | solution.py:132
  148.7 5.3 %all-to-all-done.2 = bf16[8,64,128]{2,1,0:T(8,128)(2,1)S(1)} async-done(((bf16[8,64,128]{2,1,0:T(8,128)(2,1)}), bf16[8,64,128]{2,1,0:T(8,128)(2,1)S(1)}, u32[]{:S(2)}, u32[]{:S(2)}) %all-to-all-start.2) | async-done | bytes 131104 | tf_op jit(solution)/shard_map/all_to_all | solution.py:132
  154.0 3.2 %multiply_reduce_fusion.1 = (f32[64]{0:T(128)S(1)}, f32[64,2048]{1,0:T(8,128)S(1)}) fusion(bf16[1024,2048]{1,0:T(8,128)(2,1)} %param.17, bf16[512,2048]{1,0:T(8,128)(2,1)} %param.11, s32[]{:T(128)S(6)} %select_n.3, bf16[8,64,128]{2,1,0:T(8,128)(2,1)S(1)} %all-to-all-done.2), kind=kOutput, calls=%fused_computation.12 | convolution fusion | flops 269221824 | bytes 5112068 | tf_op jit(solution)/shard_map/dot_general | solution.py:133
  157.2 0.1 multiply_convert_fusion
  157.3 0.2 broadcast_in_dim.5
  157.6 29.4 %all_to_all.40 = bf16[8,64,2048]{2,1,0:T(8,128)(2,1)S(1)} all-to-all(bf16[8,64,2048]{2,1,0:T(8,128)(2,1)S(1)} %broadcast_in_dim.5), channel_id=1, replica_groups=mesh['sp_0'=8,'sp_1'=4,'tp'=8] {'tp'}, dimensions={0} | all-to-all | bytes 4194304 | tf_op jit(solution)/shard_map/all_to_all | solution.py:91
  187.0 7.6 %fusion.11 = f32[512,1408]{1,0:T(8,128)} fusion(bf16[512,2048]{1,0:T(8,128)(2,1)S(1)} %bitcast.31, bf16[2048,1408]{1,0:T(8,128)(2,1)} %all-gather.8.cloned.1.call-done), kind=kOutput, calls=%fused_computation.30 | convolution fusion | flops 2952790016 | bytes 10747904 | tf_op jit(solution)/shard_map/dot_general | solution.py:142
  194.7 59.1 %all-gather.10.cloned.1.call-done = bf16[2048,704]{1,0:T(8,128)(2,1)} async-done(((bf16[64,704]{1,0:T(8,128)(2,1)}), bf16[2048,704]{1,0:T(8,128)(2,1)}) %all-gather.10.cloned.1.call-update) | async-done | bytes 2883600 | tf_op jit(solution)/shard_map/all_gather | solution.py:146
  253.7 4.7 %convolution_convert_fusion = bf16[512,2048]{1,0:T(8,128)(2,1)S(1)} fusion(bf16[2048,704]{1,0:T(8,128)(2,1)} %all-gather.10.cloned.1.call-done, f32[512,1408]{1,0:T(8,128)} %fusion.11), kind=kOutput, calls=%fused_computation.1 | convolution fusion | flops 1479606272 | bytes 8388608 | tf_op jit(solution)/shard_map/dot_general | solution.py:147
  258.4 34.8 %all_to_all.41 = bf16[8,64,2048]{2,1,0:T(8,128)(2,1)S(1)} all-to-all(bf16[8,64,2048]{2,1,0:T(8,128)(2,1)S(1)} %bitcast.32), channel_id=1, replica_groups=mesh['sp_0'=8,'sp_1'=4,'tp'=8] {'tp'}, dimensions={0} | all-to-all | bytes 4194304 | tf_op jit(solution)/shard_map/all_to_all | solution.py:100
  293.3 0.4 convert_reduce_fusion
  293.6 0.8 add_convert_fusion
  (17 shorter events, 0.2 us)
Async XLA Ops:
  6.5 42.1 %copy-start = (bf16[16,512]{1,0:T(8,128)(2,1)S(1)}, bf16[16,512]{1,0:T(8,128)(2,1)}, u32[]{:S(2)}) copy-start(bf16[16,512]{1,0:T(8,128)(2,1)} %constant.7.clone.1) | copy-start | bytes 49156
  6.5 40.6 %all-gather.14.cloned.1.call-start = ((), (), s32[]{:S(2)}) async-start(), calls=%async_computation.8 | async-start | bytes 1179648 | tf_op jit(solution)/shard_map/all_gather | solution.py:113
  7.3 79.2 %all-gather.12.cloned.1.call-start = ((), (), s32[]{:S(2)}) async-start(), calls=%async_computation.7 | async-start | bytes 1179648 | tf_op jit(solution)/shard_map/all_gather | solution.py:109
  8.0 179.0 %all-gather.8.cloned.1.call-start = ((), (), s32[]{:S(2)}) async-start(), calls=%async_computation.5 | async-start | bytes 5947392 | tf_op jit(solution)/shard_map/all_gather | solution.py:141
  9.8 243.9 %all-gather.10.cloned.1.call-start = ((), (), s32[]{:S(2)}) async-start(), calls=%async_computation.6 | async-start | bytes 3244032 | tf_op jit(solution)/shard_map/all_gather | solution.py:146
  121.7 13.7 %copy-start.2 = (f32[128]{0:T(128)S(1)}, f32[128]{0:T(128)}, u32[]{:S(2)}) copy-start(f32[128]{0:T(128)} %param.16) | copy-start | bytes 1540
  121.7 13.4 %all-to-all-start = ((bf16[4,128,1024]{2,1,0:T(8,128)(2,1)}), bf16[4,128,1024]{2,1,0:T(8,128)(2,1)S(1)}, u32[]{:S(2)}, u32[]{:S(2)}) async-start(bf16[4,128,1024]{2,1,0:T(8,128)(2,1)} %get-tuple-element.7), calls=%async_computation | async-start | bytes 2097152 | tf_op jit(solution)/shard_map/all_to_all | solution.py:117
  136.2 17.8 %all-to-all-start.2 = ((bf16[8,64,128]{2,1,0:T(8,128)(2,1)}), bf16[8,64,128]{2,1,0:T(8,128)(2,1)S(1)}, u32[]{:S(2)}, u32[]{:S(2)}) async-start(bf16[8,64,128]{2,1,0:T(8,128)(2,1)} %bitcast.6), calls=%async_computation.2 | async-start | bytes 262144 | tf_op jit(solution)/shard_map/all_to_all | solution.py:132
  148.7 8.5 %copy-start.1 = (f32[2048]{0:T(1024)S(1)}, f32[2048]{0:T(1024)}, u32[]{:S(2)}) copy-start(f32[2048]{0:T(1024)} %param.18) | copy-start | bytes 24580
Sparse Core Ops, SparseCore 0:
  9.0 38.0 all-gather.13
  48.9 37.4 all-gather.11
  89.0 88.2 all-gather.7
  179.7 73.9 all-gather.9

commit v2 on v1

v2 whole, which is shorter than its diff:
```python
import functools

import jax
import jax.numpy as jnp
from jax import lax
from jax.experimental import pallas as pl
from jax.experimental.pallas import tpu as pltpu
from jax.sharding import Mesh
from jax.sharding import PartitionSpec as P

HD = 64
SP = ("sp_0", "sp_1")
SP_TP = ("sp_0", "sp_1", "tp")
LOWEST = -1e30
EXTRA = 16
NZ = 8
NX = 4
MESH = pl.DeviceIdType.MESH


def spread_queries(q, out_ref, at):
    rows = q.shape[0]
    lane = lax.broadcasted_iota(jnp.int32, q.shape, 1)
    zero = jnp.zeros_like(q)
    out_ref[pl.ds(at, rows), :] = jnp.where(lane < HD, q, zero)
    out_ref[pl.ds(at + rows, rows), :] = jnp.where(lane >= HD, q, zero)


def attend_tile(q2, keys, values_t, high_ref, acc_ref):
    scores = lax.dot_general(
        keys, q2, (((1,), (1,)), ((), ())), preferred_element_type=jnp.float32
    )
    before = high_ref[...]
    after = jnp.maximum(before, jnp.max(scores, axis=0, keepdims=True))
    shrink = jnp.exp(before - after)
    weights = jnp.exp(scores - after).astype(jnp.bfloat16)
    mixed = jnp.dot(values_t, weights, preferred_element_type=jnp.float32)
    acc_ref[...] = acc_ref[...] * shrink + mixed
    high_ref[...] = after


class Ring:
    def __init__(self, axis, size, block, send, recv, steps):
        self.me = lax.axis_index(axis)
        self.axis, self.size, self.block = axis, size, block
        self.send, self.recv, self.steps = send, recv, steps

    def copy(self, way, step, at):
        target = lax.rem(self.me + (1 if way == 0 else self.size - 1), self.size)
        src, dst = self.block(way, step, at)
        return pltpu.make_async_remote_copy(
            src_ref=src,
            dst_ref=dst,
            send_sem=self.send.at[way, step],
            recv_sem=self.recv.at[way, step],
            device_id={self.axis: target},
            device_id_type=MESH,
        )

    def start(self, step):
        for way in (0, 1):
            if step < self.steps[way]:
                self.copy(way, step, 0).start()

    def arrived(self, step):
        for way in (0, 1):
            if step < self.steps[way]:
                self.copy(way, step, 1).wait_recv()

    def sent(self):
        for way in (0, 1):
            for step in range(self.steps[way]):
                self.copy(way, step, 0).wait_send()


def attention_kernel(
    q_ref, k_ref, vt_ref, w_ref, lam_ref, gain_ref,
    heads_ref, wall_ref,
    qb, kb, vb, q2, high, acc, osend, lsend, orecv, lrecv,
    q_sems, k_sems, v_sems, a_sems, az_sems, bz_sems, bx_sems, o_sems, l_sems, local_sems,
):
    z, x = lax.axis_index("sp_0"), lax.axis_index("sp_1")
    rows = q_ref.shape[0]
    width = vt_ref.shape[0]
    half = w_ref.shape[0] // 2
    quarter = half // 2
    columns = 2 * rows

    def slot(way, step):
        return 0 if step == 0 else 2 * step - 1 if way == 0 else 7 if step == 4 else 2 * step

    def k_block(way, step, at):
        return (k_ref if step + at == 0 else kb.at[slot(way, step + at)], kb.at[slot(way, step + 1)])

    def v_block(way, step, at):
        inside = vb.at[slot(way, step + at), pl.ds(0, width), :]
        return (vt_ref if step + at == 0 else inside, vb.at[slot(way, step + 1), pl.ds(0, width), :])

    def origin(way, step):
        return lax.rem(z + (NZ - step if way == 0 else step), NZ)

    def az_block(way, step, at):
        xs = pl.ds(0, NX) if step < 3 else pl.ds(0 if way == 0 else NX // 2, NX // 2)
        ref = wall_ref.at[origin(way, step + at), xs, pl.ds(0, half), :]
        return (ref, ref)

    def bz_block(way, step, at):
        rs = pl.ds(half, half) if step < 3 else pl.ds(half if way == 0 else half + quarter, quarter)
        ref = wall_ref.at[origin(way, step + at), x, rs, :]
        return (w_ref.at[pl.ds(half, half)] if step + at == 0 else ref, ref)

    def bx_block(way, step, at):
        from_x = lax.rem(x + (NX - step - at if way == 0 else step + at), NX)
        zs = pl.ds(0, NZ) if step == 0 else pl.ds(0 if way == 0 else NZ // 2, NZ // 2)
        ref = wall_ref.at[zs, from_x, pl.ds(half, half), :]
        return (ref, ref)

    kring = Ring("sp_0", NZ, k_block, k_sems.at[0], k_sems.at[1], (4, 3))
    vring = Ring("sp_0", NZ, v_block, v_sems.at[0], v_sems.at[1], (3, 4))
    azring = Ring("sp_0", NZ, az_block, az_sems.at[0], az_sems.at[1], (4, 4))
    bzring = Ring("sp_0", NZ, bz_block, bz_sems.at[0], bz_sems.at[1], (4, 4))
    bxring = Ring("sp_1", NX, bx_block, bx_sems.at[0], bx_sems.at[1], (2, 2))

    def to_peer(g, src, dst, sems):
        return pltpu.make_async_remote_copy(
            src_ref=src,
            dst_ref=dst,
            send_sem=sems.at[0, g - 1],
            recv_sem=sems.at[1, g - 1],
            device_id={"sp_1": lax.rem(x + g, NX)},
            device_id_type=MESH,
        )

    def q_copy(g):
        return to_peer(g, q_ref, qb.at[NX - 1 - g], q_sems)

    def a_copy(g, from_x):
        return to_peer(g, w_ref.at[pl.ds(0, half)], wall_ref.at[z, from_x, pl.ds(0, half), :], a_sems)

    def o_copy(g):
        return to_peer(g, osend.at[g - 1], orecv.at[g - 1], o_sems)

    def l_copy(g):
        return to_peer(g, lsend.at[g - 1], lrecv.at[g - 1], l_sems)

    barrier = pltpu.get_barrier_semaphore()
    for step in (1, NZ - 1):
        pl.semaphore_signal(
            barrier, inc=1, device_id={"sp_0": lax.rem(z + step, NZ)}, device_id_type=MESH
        )
    for step in range(1, NX):
        pl.semaphore_signal(
            barrier, inc=1, device_id={"sp_1": lax.rem(x + step, NX)}, device_id_type=MESH
        )
    pl.semaphore_wait(barrier, 2 + NX - 1)

    for g in (2, 1, 3):
        q_copy(g).start()
    kring.start(0)
    vring.start(0)
    bzring.start(0)
    for g in (2, 1, 3):
        a_copy(g, x).start()
    own_w = pltpu.make_async_copy(w_ref, wall_ref.at[z, x], local_sems.at[0])
    own_k = pltpu.make_async_copy(k_ref, kb.at[0], local_sems.at[1])
    own_v = pltpu.make_async_copy(vt_ref, vb.at[0, pl.ds(0, width), :], local_sems.at[2])
    own_w.start()
    own_k.start()
    own_v.start()
    one_row = lax.broadcasted_iota(jnp.int32, (EXTRA, rows), 0) == 0
    for i in range(NZ):
        vb[i, pl.ds(width, EXTRA), :] = jnp.where(one_row, 1.0, 0.0).astype(vb.dtype)
    spread_queries(q_ref[...], q2, 0)
    high[...] = jnp.full_like(high, LOWEST)
    acc[...] = jnp.zeros_like(acc)
    own_w.wait()
    own_k.wait()
    own_v.wait()
    for g in (1, 3, 2):
        q_copy(g).wait_recv()
    for g in range(1, NX):
        spread_queries(qb[g - 1], q2, g * columns)

    def a_arrived():
        for g in range(1, NX):
            a_copy(g, lax.rem(x + NX - g, NX)).wait_recv()

    events = {
        1: [lambda: kv_step(0), lambda: b_step(0)],
        2: [a_arrived, lambda: azring.start(0), lambda: b_step(1)],
        3: [lambda: kv_step(1), lambda: b_step(2)],
        4: [lambda: b_step(3), lambda: a_step(0)],
        5: [lambda: kv_step(2)],
        6: [lambda: a_step(1)],
        7: [lambda: kv_step(3)],
    }

    def kv_step(s):
        kring.arrived(s)
        vring.arrived(s)
        if s < 3:
            kring.start(s + 1)
            vring.start(s + 1)

    def b_step(s):
        bzring.arrived(s)
        if s < 3:
            bzring.start(s + 1)
        else:
            bxring.start(0)

    def a_step(s):
        azring.arrived(s)
        if s < 3:
            azring.start(s + 1)

    def tile(i, carry):
        for at, todo in events.items():

            @pl.when(i == at)
            def _():
                for act in todo:
                    act()

        attend_tile(q2[...], kb[i], vb[i], high, acc)
        return carry

    lax.fori_loop(0, NZ, tile, 0)

    def result(g):
        cols = pl.ds(g * columns, columns)
        totals = acc[pl.ds(width, 1), cols]
        return acc[pl.ds(0, width), cols] / totals, high[:, cols] + jnp.log(totals)

    before = None
    for g in (2, 1, 3):
        mix, lse = result(g)
        osend[g - 1] = mix.astype(osend.dtype)
        lsend[g - 1] = jnp.broadcast_to(lse, lsend.shape[1:])
        if before is not None:
            o_copy(before).start()
            l_copy(before).start()
        before = g
    mix, lse = result(0)
    o_copy(before).start()
    l_copy(before).start()
    a_step(2)
    bxring.arrived(0)
    bxring.start(1)
    for g in range(1, NX):
        o_copy(g).wait_recv()
        l_copy(g).wait_recv()
    lses = [lse] + [lrecv[g][:1] for g in range(NX - 1)]
    top = functools.reduce(jnp.maximum, lses)
    shares = [jnp.exp(one - top) for one in lses]
    mix = mix * shares[0]
    for g in range(NX - 1):
        mix = mix + orecv[g].astype(jnp.float32) * shares[g + 1]
    mix = mix / functools.reduce(jnp.add, shares)
    differ = mix[:, :rows] - lam_ref[0] * mix[:, rows:]
    square = jnp.mean(differ * differ, axis=0, keepdims=True)
    heads = differ * lax.rsqrt(square + 1e-05) * gain_ref[...]
    heads_ref[...] = heads.T.astype(heads_ref.dtype)

    azring.arrived(3)
    bxring.arrived(1)
    for ring in (kring, vring, azring, bzring, bxring):
        ring.sent()
    for g in range(1, NX):
        for copy in (q_copy(g), a_copy(g, x), o_copy(g), l_copy(g)):
            copy.wait_send()


def attention(q, k, vt, w, lambdas, gain):
    rows = q.shape[0]
    width = vt.shape[0]
    columns = NX * 2 * rows
    vmem = pl.BlockSpec(memory_space=pltpu.VMEM)
    dma = pltpu.SemaphoreType.DMA
    return pl.pallas_call(
        attention_kernel,
        out_shape=(
            jax.ShapeDtypeStruct((rows, width), jnp.bfloat16),
            jax.ShapeDtypeStruct((NZ, NX, *w.shape), jnp.bfloat16),
        ),
        in_specs=[vmem] * 4 + [pl.BlockSpec(memory_space=pltpu.SMEM), vmem],
        out_specs=[vmem] * 2,
        scratch_shapes=[
            pltpu.VMEM((NX - 1, rows, 2 * HD), jnp.bfloat16),
            pltpu.VMEM((NZ, rows, 2 * HD), jnp.bfloat16),
            pltpu.VMEM((NZ, width + EXTRA, rows), jnp.bfloat16),
            pltpu.VMEM((columns, 2 * HD), jnp.bfloat16),
            pltpu.VMEM((1, columns), jnp.float32),
            pltpu.VMEM((width + EXTRA, columns), jnp.float32),
            pltpu.VMEM((NX - 1, width, 2 * rows), jnp.bfloat16),
            pltpu.VMEM((NX - 1, 8, 2 * rows), jnp.float32),
            pltpu.VMEM((NX - 1, width, 2 * rows), jnp.bfloat16),
            pltpu.VMEM((NX - 1, 8, 2 * rows), jnp.float32),
            dma((2, NX - 1)),
            dma((2, 2, 4)),
            dma((2, 2, 4)),
            dma((2, NX - 1)),
            dma((2, 2, 4)),
            dma((2, 2, 4)),
            dma((2, 2, 2)),
            dma((2, NX - 1)),
            dma((2, NX - 1)),
            dma((3,)),
        ],
        cost_estimate=pl.CostEstimate(
            flops=30_000_000_000, bytes_accessed=8_000_000, transcendentals=16_000_000
        ),
        compiler_params=pltpu.CompilerParams(
            vmem_limit_bytes=60 * 2**20, collective_id=0, has_side_effects=True
        ),
    )(q, k, vt, w, lambdas, gain)


def laid_out(parts, dim):
    parts = jnp.moveaxis(parts, 0, dim)
    dims = parts.shape
    return parts.reshape(*dims[:dim], dims[dim] * dims[dim + 1], *dims[dim + 2 :])


def gather_directly(shard, axis, dim):
    length = lax.axis_size(axis)
    parts = lax.all_to_all(
        jnp.broadcast_to(shard[None], (length, *shard.shape)), axis, 0, 0, tiled=True
    )
    return laid_out(parts, dim)


def summed_on_arrival(shard, axis):
    length = lax.axis_size(axis)
    parts = shard.reshape(length, shard.shape[0] // length, shard.shape[1])
    arrived = lax.all_to_all(parts, axis, split_axis=0, concat_axis=0, tiled=True)
    return arrived.astype(jnp.float32).sum(axis=0)


def per_device(
    residual, queries, key_pairs, values, lambdas, head_gain, w_out, norm_gain, w_gate, w_up, w_down
):
    local_rows = queries.shape[0]
    scaled_q = queries * jnp.bfloat16(HD**-0.5)
    joined = jnp.concatenate([w_gate, w_up], axis=1)
    down_t = lax.all_gather(w_down.T, SP, axis=0, tiled=True)
    heads_out, w_all = attention(
        scaled_q, key_pairs, values.T, joined, lambdas, head_gain[:, None]
    )
    w_all = w_all.reshape(-1, w_all.shape[-1])
    tp_index = lax.axis_index("tp")
    own_rows = local_rows // lax.axis_size("tp")
    own_begin = tp_index * own_rows
    token_heads = lax.all_to_all(heads_out, "tp", split_axis=0, concat_axis=1, tiled=True)
    projected = jnp.dot(token_heads, w_out, preferred_element_type=jnp.float32)
    residual_own = lax.dynamic_slice_in_dim(residual, own_begin, own_rows, 0)
    hidden_own = (residual_own.astype(jnp.float32) + projected).astype(jnp.bfloat16)
    stream_f = hidden_own.astype(jnp.float32)
    scaled = stream_f * lax.rsqrt(jnp.mean(stream_f * stream_f, axis=-1, keepdims=True) + 1e-05)
    normed_rows = gather_directly((scaled * norm_gain).astype(jnp.bfloat16), "tp", 0)
    unit_width = w_gate.shape[1]
    both_sums = jnp.dot(normed_rows, w_all, preferred_element_type=jnp.float32)
    gate_sum = both_sums[:, :unit_width]
    up_sum = both_sums[:, unit_width:]
    hidden_units = (jax.nn.silu(gate_sum) * up_sum).astype(jnp.bfloat16)
    ffn_part = lax.dot_general(
        hidden_units, down_t, (((1,), (1,)), ((), ())), preferred_element_type=jnp.float32
    )
    ffn_out = summed_on_arrival(ffn_part.astype(jnp.bfloat16), "tp")
    return (hidden_own.astype(jnp.float32) + ffn_out).astype(jnp.bfloat16)


def solution(mesh):
    torus = Mesh(mesh.devices.reshape(8, 4, mesh.shape["tp"]), ("sp_0", "sp_1", "tp"))
    return jax.shard_map(
        per_device,
        mesh=torus,
        in_specs=(
            P(SP, None),
            P(SP, "tp"),
            P(SP, "tp"),
            P(SP, "tp"),
            P("tp"),
            P(),
            P(),
            P(),
            P(SP, "tp"),
            P(SP, "tp"),
            P("tp", SP),
        ),
        out_specs=P(SP_TP, None),
        check_vma=False,
    )
```

time: 301 us -> 207 us (0.69)
  waiting for transfers between devices: 135 us -> 5.97 us
  Pallas kernels: 26.4 us -> 104 us
  blocking collectives: 85.9 us -> 59.4 us
  starting transfers between devices: 16.2 us -> 5.09 us
  matrix products: 15.6 us -> 10.3 us
    pallas_call x1, Pallas kernels: 26.4 us -> 104 us  [attention(): pl.pallas_call(attention_kernel, out_shape=(jax.ShapeDtypeStruct((rows, w...]
    all_gather x3 -> x0, waiting for transfers between devices: 59.7 us -> none  [the longest x1 36.6 us: per_device(): k_all = lax.all_gather(key_pairs, 'sp_0', axis=0)]
    all_gather x1, waiting for transfers between devices: 59.1 us -> 0.02 us  [per_device(): down_t = lax.all_gather(w_down.T, SP, axis=0, tiled=True)]
    all_gather x1 -> x0, blocking collectives: 12.8 us -> none  [per_device(): q_all = lax.all_gather(scaled_q, 'sp_1', axis=0)]
    all_to_all x1 -> x0, waiting for transfers between devices: 8.93 us -> none  [per_device(): lax.all_to_all(mixed_part, 'sp_1', 0, 0, tiled=True).astype(jnp.float32)]
    all_to_all x1 -> x0, blocking collectives: 8.89 us -> none  [per_device(): lse_part = lax.all_to_all(lse_part, 'sp_1', 0, 0, tiled=True)[:, :1]]
    all_to_all x1, starting transfers between devices: 12.5 us -> 5.09 us  [per_device(): lax.all_to_all(heads_out, 'tp', split_axis=0, concat_axis=1, tiled=True)]
    all_to_all x1, blocking collectives: 34.8 us -> 29.7 us  [summed_on_arrival(): lax.all_to_all(parts, axis, split_axis=0, concat_axis=0, tiled=True)]
  transfers between devices with their start and end apart: 6 -> 2, of which waited for: 5 -> 1; matrix products, arithmetic and copies ran while one was open for 6% -> 6% of each run, Pallas kernels for 9% -> 50%
where the time goes in v2:
time: 207 us
  Pallas kernels  104 us (50%)
  blocking collectives  59.4 us (29%)
  between operations  14.1 us (7%)
  matrix products  10.3 us (5%)
  waiting for transfers between devices  5.97 us (3%)
  starting transfers between devices  5.09 us (2%)
  other arithmetic  4.52 us (2%)
  local copies, waits for them, and re-layouts  3.29 us (2%)
    pallas_call x1, Pallas kernels, attention(): pl.pallas_call(attention_kernel, out_shape=(jax.ShapeDtypeStruct((rows, w...  104 us
    all_to_all x1, blocking collectives, gather_directly(): lax.all_to_all(jnp.broadcast_to(shard[None], (length, *shard.shape)), axi...  29.7 us
    all_to_all x1, blocking collectives, summed_on_arrival(): lax.all_to_all(parts, axis, split_axis=0, concat_axis=0, tiled=True)  29.7 us
    all_to_all x1, waiting for transfers between devices, per_device(): lax.all_to_all(heads_out, 'tp', split_axis=0, concat_axis=1, tiled=True)  5.24 us
    all_to_all x1, starting transfers between devices, per_device(): lax.all_to_all(heads_out, 'tp', split_axis=0, concat_axis=1, tiled=True)  5.09 us
  transfers between devices with their start and end apart: 2, of which 1 were waited for; matrix products, arithmetic and copies ran while one was open for 6% of the time, Pallas kernels for 50%

profile of v2, /device:TPU:1, one launch (start us, length us, event | category | flops | bytes accessed | tf_op | source)
XLA Modules:
  0.0 206.7 jit_solution(13576024028260468926)
XLA Ops:
  6.5 0.0 all-gather.2.cloned.1.call-start
  6.5 0.7 all-gather.2.cloned.1.call-update
  7.3 1.7 copy.17
  8.9 1.6 broadcast_multiply_fusion.q_ref
  10.5 1.4 copy.18.gain_ref
  12.5 1.7 pad_maximum_fusion.w_ref
  14.2 103.9 %shard_map.109 = (bf16[512,128]{1,0:T(8,128)(2,1)}, bf16[8,4,64,1408]{3,2,1,0:T(8,128)(2,1)}) custom-call(bf16[512,128]{1,0:T(8,128)(2,1)} %broadcast_multiply_fusion.q_ref, bf16[512,128]{1,0:T(8,128)(2,1)} %k_ref.1, bf16[128,512]{1,0:T(8,128)(2,1)} %bitcast.24, bf16[64,1408]{1,0:T(8,128)(2,1)} %pad_maximum_fusion.w_ref, f32[1]{0:T(128)S(6)} %copy.27.lam_ref, ...), custom_call_target="tpu_custom_call" | custom-call | flops 30000001024 | bytes 8000000 | tf_op jit(solution)/shard_map/pallas_call | solution.py:280
  118.2 5.1 %all-to-all-start = ((bf16[8,64,128]{2,1,0:T(8,128)(2,1)}), bf16[8,64,128]{2,1,0:T(8,128)(2,1)S(1)}, u32[]{:S(2)}, u32[]{:S(2)}) async-start(bf16[8,64,128]{2,1,0:T(8,128)(2,1)} %bitcast.23), calls=%async_computation | async-start | bytes 262144 | tf_op jit(solution)/shard_map/all_to_all | solution.py:354
  123.3 0.0 copy-start
  123.3 5.2 %all-to-all-done = bf16[8,64,128]{2,1,0:T(8,128)(2,1)S(1)} async-done(((bf16[8,64,128]{2,1,0:T(8,128)(2,1)}), bf16[8,64,128]{2,1,0:T(8,128)(2,1)S(1)}, u32[]{:S(2)}, u32[]{:S(2)}) %all-to-all-start) | async-done | bytes 131104 | tf_op jit(solution)/shard_map/all_to_all | solution.py:354
  128.5 3.2 %multiply_reduce_fusion = (f32[64]{0:T(128)S(1)}, f32[64,2048]{1,0:T(8,128)S(1)}) fusion(bf16[1024,2048]{1,0:T(8,128)(2,1)} %param.17, bf16[512,2048]{1,0:T(8,128)(2,1)} %param.11, s32[]{:T(128)S(6)} %select_n.3, bf16[8,64,128]{2,1,0:T(8,128)(2,1)S(1)} %all-to-all-done), kind=kOutput, calls=%fused_computation.10 | convolution fusion | flops 269221824 | bytes 5112068 | tf_op jit(solution)/shard_map/dot_general | solution.py:355
  131.7 0.0 copy-done
  131.7 0.1 multiply_convert_fusion
  131.8 0.0 copy-start.1
  131.8 0.2 broadcast_in_dim.5
  132.1 29.7 %all_to_all.29 = bf16[8,64,2048]{2,1,0:T(8,128)(2,1)S(1)} all-to-all(bf16[8,64,2048]{2,1,0:T(8,128)(2,1)S(1)} %broadcast_in_dim.5), channel_id=1, replica_groups=mesh['sp_0'=8,'sp_1'=4,'tp'=8] {'tp'}, dimensions={0} | all-to-all | bytes 4194304 | tf_op jit(solution)/shard_map/all_to_all | solution.py:327
  161.8 0.0 copy-done.1
  161.8 3.4 %fusion.8 = f32[512,1408]{1,0:T(8,128)S(1)} fusion(bf16[512,2048]{1,0:T(8,128)(2,1)S(1)} %bitcast.21, bf16[2048,1408]{1,0:T(8,128)(2,1)S(1)} %bitcast.27), kind=kOutput, calls=%fused_computation.17 | convolution fusion | flops 2952790016 | bytes 10747904 | tf_op jit(solution)/shard_map/dot_general | solution.py:362
  165.2 0.0 all-gather.2.cloned.1.call-done
  165.3 3.8 %convolution_convert_fusion = bf16[512,2048]{1,0:T(8,128)(2,1)S(1)} fusion(bf16[2048,704]{1,0:T(8,128)(2,1)} %all-gather.2.cloned.1.call-done, f32[512,1408]{1,0:T(8,128)S(1)} %fusion.8), kind=kOutput, calls=%fused_computation.1 | convolution fusion | flops 1479606272 | bytes 8126464 | tf_op jit(solution)/shard_map/dot_general | solution.py:366
  169.0 29.7 %all_to_all.30 = bf16[8,64,2048]{2,1,0:T(8,128)(2,1)S(1)} all-to-all(bf16[8,64,2048]{2,1,0:T(8,128)(2,1)S(1)} %bitcast.22), channel_id=1, replica_groups=mesh['sp_0'=8,'sp_1'=4,'tp'=8] {'tp'}, dimensions={0} | all-to-all | bytes 4194304 | tf_op jit(solution)/shard_map/all_to_all | solution.py:336
  198.7 0.4 convert_reduce_fusion
  199.0 0.8 add_convert_fusion
  (1 shorter events, 0.0 us)
Async XLA Ops:
  6.5 158.7 %all-gather.2.cloned.1.call-start = ((), (), s32[]{:S(2)}) async-start(), calls=%async_computation.3 | async-start | bytes 3244032 | tf_op jit(solution)/shard_map/all_gather | solution.py:346
  118.2 10.3 %all-to-all-start = ((bf16[8,64,128]{2,1,0:T(8,128)(2,1)}), bf16[8,64,128]{2,1,0:T(8,128)(2,1)S(1)}, u32[]{:S(2)}, u32[]{:S(2)}) async-start(bf16[8,64,128]{2,1,0:T(8,128)(2,1)} %bitcast.23), calls=%async_computation | async-start | bytes 262144 | tf_op jit(solution)/shard_map/all_to_all | solution.py:354
  123.3 8.4 %copy-start = (f32[2048]{0:T(1024)S(1)}, f32[2048]{0:T(1024)}, u32[]{:S(2)}) copy-start(f32[2048]{0:T(1024)} %param.18) | copy-start | bytes 24580
  131.8 30.0 %copy-start.1 = (bf16[8,4,64,1408]{3,2,1,0:T(8,128)(2,1)S(1)}, bf16[8,4,64,1408]{3,2,1,0:T(8,128)(2,1)}, u32[]{:S(2)}) copy-start(bf16[8,4,64,1408]{3,2,1,0:T(8,128)(2,1)} %get-tuple-element.8) | copy-start | bytes 17301508
Sparse Core Ops, SparseCore 0:
  9.9 94.2 all-gather.1

commit v3 on v2

v3 whole, which is shorter than its diff:
```python
import functools

import jax
import jax.numpy as jnp
from jax import lax
from jax.experimental import pallas as pl
from jax.experimental.pallas import tpu as pltpu
from jax.sharding import Mesh
from jax.sharding import PartitionSpec as P

HD = 64
SP = ("sp_0", "sp_1")
SP_TP = ("sp_0", "sp_1", "tp")
LOWEST = -1e30
EXTRA = 16
NZ = 8
NX = 4
NY = 4
NT = 8
MESH = pl.DeviceIdType.MESH


def spread_queries(q, out_ref, at):
    rows = q.shape[0]
    lane = lax.broadcasted_iota(jnp.int32, q.shape, 1)
    zero = jnp.zeros_like(q)
    out_ref[pl.ds(at, rows), :] = jnp.where(lane < HD, q, zero)
    out_ref[pl.ds(at + rows, rows), :] = jnp.where(lane >= HD, q, zero)


def attend_tile(q2, keys, values_t, high_ref, acc_ref):
    scores = lax.dot_general(
        keys, q2, (((1,), (1,)), ((), ())), preferred_element_type=jnp.float32
    )
    before = high_ref[...]
    after = jnp.maximum(before, jnp.max(scores, axis=0, keepdims=True))
    shrink = jnp.exp(before - after)
    weights = jnp.exp(scores - after).astype(jnp.bfloat16)
    mixed = jnp.dot(values_t, weights, preferred_element_type=jnp.float32)
    acc_ref[...] = acc_ref[...] * shrink + mixed
    high_ref[...] = after


class Ring:
    def __init__(self, target, block, send, recv, steps):
        self.target, self.block = target, block
        self.send, self.recv, self.steps = send, recv, steps

    def copy(self, way, step, at):
        src, dst = self.block(way, step, at)
        return pltpu.make_async_remote_copy(
            src_ref=src,
            dst_ref=dst,
            send_sem=self.send.at[way, step],
            recv_sem=self.recv.at[way, step],
            device_id=self.target(way),
            device_id_type=MESH,
        )

    def start(self, step):
        for way in (0, 1):
            if step < self.steps[way]:
                self.copy(way, step, 0).start()

    def arrived(self, step):
        for way in (0, 1):
            if step < self.steps[way]:
                self.copy(way, step, 1).wait_recv()

    def sent(self):
        for way in (0, 1):
            for step in range(self.steps[way]):
                self.copy(way, step, 0).wait_send()


class Gather:
    def __init__(self, shard, whole, z, x, z_target, x_target, z_sems, one_sems, two_sems):
        self.shard, self.whole, self.z, self.x = shard, whole, z, x
        self.x_target, self.one, self.two = x_target, one_sems, two_sems
        self.rows = shard.shape[0]
        self.ring = Ring(z_target, self.z_block, z_sems.at[0], z_sems.at[1], (4, 4))

    def origin(self, index):
        step = (index + 1) // 2
        return lax.rem(self.z + (NZ - step if index % 2 else step), NZ)

    def z_block(self, way, step, at):
        half = self.rows // 2
        rows = pl.ds(0, self.rows) if step < 3 else pl.ds(half * way, half)
        origin = lax.rem(self.z + (NZ - step - at if way == 0 else step + at), NZ)
        ref = self.whole(origin, self.x, rows)
        return (self.shard if step + at == 0 else ref, ref)

    def along_x(self, src, dst, sems, way, index):
        return pltpu.make_async_remote_copy(
            src_ref=src,
            dst_ref=dst,
            send_sem=sems.at[0, way, index],
            recv_sem=sems.at[1, way, index],
            device_id=self.x_target(way),
            device_id_type=MESH,
        )

    def hop(self, number, way, index, at):
        step = number - 1 + at
        from_x = lax.rem(self.x + (NX - step if way == 0 else step), NX)
        ref = self.whole(self.origin(index), from_x, pl.ds(0, self.rows))
        own = number == 1 and at == 0 and index == 0
        sems = self.one if number == 1 else self.two
        return self.along_x(self.shard if own else ref, ref, sems, way, index)

    def members(self, k):
        return [0] if k == 0 else [7] if k == 4 else [2 * k - 1, 2 * k]

    def second_way(self, index):
        return 0 if index in (0, 1, 3, 5) else 1

    def step(self, k):
        if k > 0:
            self.ring.arrived(k - 1)
        if k < 4:
            self.ring.start(k)
        for index in self.members(k):
            for way in (0, 1):
                self.hop(1, way, index, 0).start()

    def forward(self, k):
        for index in self.members(k):
            for way in (0, 1):
                self.hop(1, way, index, 1).wait_recv()
            self.hop(2, self.second_way(index), index, 0).start()

    def done(self):
        for index in range(NZ):
            self.hop(2, self.second_way(index), index, 1).wait_recv()

    def sent(self):
        self.ring.sent()
        for index in range(NZ):
            for way in (0, 1):
                self.hop(1, way, index, 0).wait_send()
            self.hop(2, self.second_way(index), index, 0).wait_send()


def layer_kernel(
    q_ref, k_ref, vt_ref, w_ref, wd_ref, lam_ref, gain_ref, norm_gain_ref, res_ref, wout_ref,
    out_ref,
    qb, kb, vb, q2, high, acc, osend, lsend, orecv, lrecv, orelay,
    wall, down, wout, res, heads, th, normed, hidden, units, parts, pb, pr, fs, fr, relay,
    q_sems, k_sems, v_sems, ax_sems, az_sems, bz_sems, b1_sems, b2_sems,
    cz_sems, c1_sems, c2_sems, o_sems, l_sems, or_sems, local_sems,
    h_sems, y_sems, p_sems, c_sems, r_sems, rr_sems,
):
    z, x, t = lax.axis_index("sp_0"), lax.axis_index("sp_1"), lax.axis_index("tp")
    y, core = t // 2, lax.rem(t, 2)
    rows = q_ref.shape[0]
    width = vt_ref.shape[0]
    half = w_ref.shape[0] // 2
    columns = 2 * rows
    own = rows // NT
    unit_width = wd_ref.shape[1]

    def z_target(way):
        return {"sp_0": lax.rem(z + (1 if way == 0 else NZ - 1), NZ)}

    def x_target(way):
        return {"sp_1": lax.rem(x + (1 if way == 0 else NX - 1), NX)}

    def chip(offset):
        return lax.rem(y + offset, NY)

    def y_target(way):
        return {"tp": chip(1 if way == 0 else NY - 1) * 2 + core}

    partner = {"tp": t + 1 - 2 * core}

    def slot(way, step):
        return 0 if step == 0 else 2 * step - 1 if way == 0 else 7 if step == 4 else 2 * step

    def k_block(way, step, at):
        src = k_ref if step + at == 0 else kb.at[slot(way, step + at)]
        return (src, kb.at[slot(way, step + 1)])

    def v_block(way, step, at):
        inside = vb.at[slot(way, step + at), pl.ds(0, width), :]
        src = vt_ref if step + at == 0 else inside
        return (src, vb.at[slot(way, step + 1), pl.ds(0, width), :])

    def q_block(way, step, at):
        part = pl.ds(0, rows) if step == 0 else pl.ds(way * (rows // 2), rows // 2)
        place = lambda hops: (2 if way == 0 else 0) if hops == 1 else 1
        src = q_ref if step + at == 0 else qb.at[place(step + at), part, :]
        return (src, qb.at[place(step + 1), part, :])

    def ax_block(way, step, at):
        part = pl.ds(0, half) if step == 0 else pl.ds(way * (half // 2), half // 2)
        from_x = lax.rem(x + (NX - step - at if way == 0 else step + at), NX)
        ref = wall.at[z, from_x, part, :]
        return (w_ref.at[pl.ds(0, half)] if step + at == 0 else ref, ref)

    def az_block(way, step, at):
        xs = pl.ds(0, NX) if step < 3 else pl.ds(0 if way == 0 else NX // 2, NX // 2)
        origin = lax.rem(z + (NZ - step - at if way == 0 else step + at), NZ)
        ref = wall.at[origin, xs, pl.ds(0, half), :]
        return (ref, ref)

    def b_whole(from_z, from_x, part):
        return wall.at[from_z, from_x, pl.ds(half + part.start, part.size), :]

    def c_whole(from_z, from_x, part):
        return down.at[from_z, from_x, part, :]

    def o_block(way, step, at):
        part = pl.ds(way * (width // 2), width // 2)
        if step == 0:
            return (osend.at[1, part, :], orelay.at[way])
        return (orelay.at[way], orecv.at[1, part, :])

    kring = Ring(z_target, k_block, k_sems.at[0], k_sems.at[1], (4, 3))
    vring = Ring(z_target, v_block, v_sems.at[0], v_sems.at[1], (3, 4))
    qring = Ring(x_target, q_block, q_sems.at[0], q_sems.at[1], (2, 2))
    axring = Ring(x_target, ax_block, ax_sems.at[0], ax_sems.at[1], (2, 2))
    azring = Ring(z_target, az_block, az_sems.at[0], az_sems.at[1], (4, 4))
    oring = Ring(x_target, o_block, or_sems.at[0], or_sems.at[1], (2, 2))
    later = Gather(
        w_ref.at[pl.ds(half, half)], b_whole, z, x, z_target, x_target, bz_sems, b1_sems, b2_sems
    )
    lowest = Gather(wd_ref, c_whole, z, x, z_target, x_target, cz_sems, c1_sems, c2_sems)

    def x_peer(g, src, dst, sems):
        return pltpu.make_async_remote_copy(
            src_ref=src,
            dst_ref=dst,
            send_sem=sems.at[0, g - 1],
            recv_sem=sems.at[1, g - 1],
            device_id={"sp_1": lax.rem(x + g, NX)},
            device_id_type=MESH,
        )

    def o_copy(g):
        return x_peer(g, osend.at[g - 1], orecv.at[g - 1], o_sems)

    def l_copy(g):
        return x_peer(g, lsend.at[g - 1], lrecv.at[g - 1], l_sems)

    barrier = pltpu.get_barrier_semaphore()
    greeted = [{"sp_0": lax.rem(z + s, NZ)} for s in (1, NZ - 1)]
    greeted += [{"sp_1": lax.rem(x + s, NX)} for s in range(1, NX)]
    greeted += [{"tp": lax.rem(t + s, NT)} for s in range(1, NT)]
    for device in greeted:
        pl.semaphore_signal(barrier, inc=1, device_id=device, device_id_type=MESH)
    pl.semaphore_wait(barrier, len(greeted))

    qring.start(0)
    kring.start(0)
    vring.start(0)
    axring.start(0)
    later.step(0)
    locals_ = [
        pltpu.make_async_copy(src, dst, local_sems.at[i])
        for i, (src, dst) in enumerate(
            (
                (k_ref, kb.at[0]),
                (vt_ref, vb.at[0, pl.ds(0, width), :]),
                (w_ref, wall.at[z, x]),
                (wd_ref, down.at[z, x]),
                (res_ref.at[pl.ds(pl.multiple_of(t * own, own), own), :], res),
                (wout_ref, wout),
            )
        )
    ]
    for copy in locals_:
        copy.start()
    one_row = lax.broadcasted_iota(jnp.int32, (EXTRA, rows), 0) == 0
    for i in range(NZ):
        vb[i, pl.ds(width, EXTRA), :] = jnp.where(one_row, 1.0, 0.0).astype(vb.dtype)
    spread_queries(q_ref[...], q2, 0)
    high[...] = jnp.full_like(high, LOWEST)
    acc[...] = jnp.zeros_like(acc)
    for copy in locals_[:4]:
        copy.wait()

    def group_tile(g):
        cols = pl.ds(g * columns, columns)
        attend_tile(q2[cols, :], kb[0], vb[0], high.at[:, cols], acc.at[:, cols])

    def kv_step(s):
        kring.arrived(s)
        vring.arrived(s)
        if s < 3:
            kring.start(s + 1)
            vring.start(s + 1)

    def a_step(s):
        azring.arrived(s)
        if s < 3:
            azring.start(s + 1)

    group_tile(0)
    qring.arrived(0)
    qring.start(1)
    axring.arrived(0)
    axring.start(1)
    for g in (1, 3):
        spread_queries(qb[g - 1], q2, g * columns)
        group_tile(g)
    kv_step(0)
    later.step(1)
    later.forward(0)
    qring.arrived(1)
    spread_queries(qb[1], q2, 2 * columns)
    group_tile(2)
    axring.arrived(1)
    azring.start(0)

    events = {
        2: [lambda: later.step(2), lambda: later.forward(1)],
        3: [lambda: kv_step(1)],
        4: [lambda: a_step(0), lambda: later.step(3), lambda: later.forward(2)],
        5: [lambda: kv_step(2)],
        6: [lambda: later.step(4), lambda: later.forward(3), lambda: a_step(1), lambda: lowest.step(0)],
        7: [lambda: kv_step(3)],
    }

    def tile(i, carry):
        for at, todo in events.items():

            @pl.when(i == at)
            def _():
                for act in todo:
                    act()

        attend_tile(q2[...], kb[i], vb[i], high, acc)
        return carry

    lax.fori_loop(1, NZ, tile, 0)

    def result(g):
        cols = pl.ds(g * columns, columns)
        totals = acc[pl.ds(width, 1), cols]
        return acc[pl.ds(0, width), cols] / totals, high[:, cols] + jnp.log(totals)

    def stored(g):
        mix, lse = result(g)
        osend[g - 1] = mix.astype(osend.dtype)
        lsend[g - 1] = jnp.broadcast_to(lse, lsend.shape[1:])

    stored(2)
    lowest.step(1)
    lowest.forward(0)
    stored(1)
    oring.start(0)
    l_copy(2).start()
    stored(3)
    o_copy(1).start()
    l_copy(1).start()
    mix, lse = result(0)
    o_copy(3).start()
    l_copy(3).start()
    later.forward(4)
    a_step(2)
    oring.arrived(0)
    oring.start(1)
    lowest.step(2)
    lowest.forward(1)
    for g in (1, 3):
        o_copy(g).wait_recv()
    for g in range(1, NX):
        l_copy(g).wait_recv()
    oring.arrived(1)
    lses = [lse] + [lrecv[g][:1] for g in range(NX - 1)]
    top = functools.reduce(jnp.maximum, lses)
    shares = [jnp.exp(one - top) for one in lses]
    mix = mix * shares[0]
    for g in range(NX - 1):
        mix = mix + orecv[g].astype(jnp.float32) * shares[g + 1]
    mix = mix / functools.reduce(jnp.add, shares)
    differ = mix[:, :rows] - lam_ref[0] * mix[:, rows:]
    square = jnp.mean(differ * differ, axis=0, keepdims=True)
    mine = differ * lax.rsqrt(square + 1e-05) * gain_ref[...]
    heads[...] = mine.T.astype(heads.dtype)
    lowest.step(3)
    lowest.forward(2)

    def own_rows(index):
        return pl.ds(pl.multiple_of(index * own, own), own)

    def h_copy(d, to, home):
        return pltpu.make_async_remote_copy(
            src_ref=heads.at[own_rows(to), :],
            dst_ref=th.at[home],
            send_sem=h_sems.at[0, d - 1],
            recv_sem=h_sems.at[1, d - 1],
            device_id={"tp": to},
            device_id_type=MESH,
        )

    for d in range(1, NT):
        h_copy(d, lax.rem(t + d, NT), t).start()
    th[t] = heads[own_rows(t), :]
    lowest.step(4)
    lowest.forward(3)
    for copy in locals_[4:]:
        copy.wait()
    for d in range(1, NT):
        h_copy(d, lax.rem(t + d, NT), lax.rem(t + NT - d, NT)).wait_recv()
    token_heads = jnp.concatenate([th[h] for h in range(NT)], axis=1)
    projected = jnp.dot(token_heads, wout[...], preferred_element_type=jnp.float32)
    stream = (res[...].astype(jnp.float32) + projected).astype(jnp.bfloat16)
    hidden[...] = stream
    stream = stream.astype(jnp.float32)
    scale = lax.rsqrt(jnp.mean(stream * stream, axis=-1, keepdims=True) + 1e-05)
    normed[t] = (stream * scale * norm_gain_ref[...]).astype(normed.dtype)

    def y_block(way, step, at):
        part = pl.ds(0, own) if step == 0 else pl.ds(way * (own // 2), own // 2)
        ref = normed.at[chip(NY - step - at if way == 0 else step + at) * 2 + core, part, :]
        return (ref, ref)

    yring = Ring(y_target, y_block, y_sems.at[0], y_sems.at[1], (2, 2))
    shared = ((0, 0, own), (NY - 1, 0, own), (1, 0, own), (2, 0, own // 2), (2, own // 2, own // 2))

    def p_copy(number, of_core):
        offset, first, count = shared[number]
        ref = normed.at[chip(offset) * 2 + of_core, pl.ds(first, count), :]
        return pltpu.make_async_remote_copy(
            src_ref=ref,
            dst_ref=ref,
            send_sem=p_sems.at[0, number],
            recv_sem=p_sems.at[1, number],
            device_id=partner,
            device_id_type=MESH,
        )

    yring.start(0)
    p_copy(0, core).start()
    lowest.forward(4)
    yring.arrived(0)
    yring.start(1)
    p_copy(1, core).start()
    p_copy(2, core).start()
    yring.arrived(1)
    p_copy(3, core).start()
    p_copy(4, core).start()
    later.done()
    azring.arrived(3)
    for number in range(len(shared)):
        p_copy(number, 1 - core).wait_recv()
    sums = jnp.dot(
        normed[...].reshape(rows, -1),
        wall[...].reshape(-1, wall.shape[-1]),
        preferred_element_type=jnp.float32,
    )
    gate, up = sums[:, :unit_width], sums[:, unit_width:]
    gated = gate / (1.0 + jnp.exp(-gate)) * up
    units[...] = gated.astype(units.dtype).reshape(units.shape)
    lowest.done()

    def piece(offset):
        lhs = units[pl.ds(chip(offset) * 2, 2)].reshape(2 * own, unit_width)
        part = lax.dot_general(
            lhs,
            down[...].reshape(-1, unit_width),
            (((1,), (1,)), ((), ())),
            preferred_element_type=jnp.float32,
        )
        parts[offset] = part.reshape(parts.shape[1:])
        pb[offset] = parts[offset, 1 - core].astype(pb.dtype)

    def pair_copy(offset):
        return pltpu.make_async_remote_copy(
            src_ref=pb.at[offset],
            dst_ref=pr.at[offset],
            send_sem=c_sems.at[0, offset],
            recv_sem=c_sems.at[1, offset],
            device_id=partner,
            device_id_type=MESH,
        )

    def paired(offset):
        pair_copy(offset).wait_recv()
        return parts[offset, core] + pr[offset].astype(jnp.float32)

    def r_block(way, step, at):
        return (fs.at[1 if way == 0 else NY - 1], fr.at[way])

    def rr_block(way, step, at):
        part = pl.ds(way * (own // 2), own // 2)
        if step == 0:
            return (fs.at[2, part, :], relay.at[way])
        return (relay.at[way], fr.at[2, part, :])

    rring = Ring(y_target, r_block, r_sems.at[0], r_sems.at[1], (1, 1))
    rrring = Ring(y_target, rr_block, rr_sems.at[0], rr_sems.at[1], (2, 2))
    piece(2)
    piece(3)
    pair_copy(2).start()
    piece(1)
    pair_copy(3).start()
    fs[2] = paired(2).astype(fs.dtype)
    piece(0)
    pair_copy(1).start()
    rrring.start(0)
    fs[3] = paired(3).astype(fs.dtype)
    fs[1] = paired(1).astype(fs.dtype)
    pair_copy(0).start()
    rring.start(0)
    total = hidden[...].astype(jnp.float32) + paired(0)
    rrring.arrived(0)
    rrring.start(1)
    rring.arrived(0)
    total = total + fr[0].astype(jnp.float32) + fr[1].astype(jnp.float32)
    rrring.arrived(1)
    out_ref[...] = (total + fr[2].astype(jnp.float32)).astype(out_ref.dtype)

    for ring in (kring, vring, qring, axring, azring, oring, later, lowest, yring, rring, rrring):
        ring.sent()
    for g in (1, 3):
        o_copy(g).wait_send()
    for g in range(1, NX):
        l_copy(g).wait_send()
    for d in range(1, NT):
        h_copy(d, lax.rem(t + d, NT), t).wait_send()
    for number in range(len(shared)):
        p_copy(number, core).wait_send()
    for offset in range(NY):
        pair_copy(offset).wait_send()


def layer(q, k, vt, w, wd, lambdas, gain, norm_gain, residual, w_out):
    rows = q.shape[0]
    width = vt.shape[0]
    model = residual.shape[1]
    columns = NX * 2 * rows
    own = rows // NT
    units = wd.shape[1]
    vmem = pl.BlockSpec(memory_space=pltpu.VMEM)
    smem = pl.BlockSpec(memory_space=pltpu.SMEM)
    hbm = pl.BlockSpec(memory_space=pl.ANY)
    dma = pltpu.SemaphoreType.DMA
    short, long = jnp.bfloat16, jnp.float32
    return pl.pallas_call(
        layer_kernel,
        out_shape=jax.ShapeDtypeStruct((own, model), short),
        in_specs=[vmem] * 5 + [smem, vmem, vmem, hbm, hbm],
        out_specs=vmem,
        scratch_shapes=[
            pltpu.VMEM((NX - 1, rows, 2 * HD), short),
            pltpu.VMEM((NZ, rows, 2 * HD), short),
            pltpu.VMEM((NZ, width + EXTRA, rows), short),
            pltpu.VMEM((columns, 2 * HD), short),
            pltpu.VMEM((1, columns), long),
            pltpu.VMEM((width + EXTRA, columns), long),
            pltpu.VMEM((NX - 1, width, 2 * rows), short),
            pltpu.VMEM((NX - 1, 8, 2 * rows), long),
            pltpu.VMEM((NX - 1, width, 2 * rows), short),
            pltpu.VMEM((NX - 1, 8, 2 * rows), long),
            pltpu.VMEM((2, width // 2, 2 * rows), short),
            pltpu.VMEM((NZ, NX, *w.shape), short),
            pltpu.VMEM((NZ, NX, *wd.shape), short),
            pltpu.VMEM(w_out.shape, short),
            pltpu.VMEM((own, model), short),
            pltpu.VMEM((rows, width), short),
            pltpu.VMEM((NT, own, width), short),
            pltpu.VMEM((NT, own, model), short),
            pltpu.VMEM((own, model), short),
            pltpu.VMEM((NT, own, units), short),
            pltpu.VMEM((NY, 2, own, model), long),
            pltpu.VMEM((NY, own, model), short),
            pltpu.VMEM((NY, own, model), short),
            pltpu.VMEM((NY, own, model), short),
            pltpu.VMEM((NY - 1, own, model), short),
            pltpu.VMEM((2, own // 2, model), short),
            dma((2, 2, 2)),
            dma((2, 2, 4)),
            dma((2, 2, 4)),
            dma((2, 2, 2)),
            dma((2, 2, 4)),
            dma((2, 2, 4)),
            dma((2, 2, NZ)),
            dma((2, 2, NZ)),
            dma((2, 2, 4)),
            dma((2, 2, NZ)),
            dma((2, 2, NZ)),
            dma((2, NX - 1)),
            dma((2, NX - 1)),
            dma((2, 2, 2)),
            dma((6,)),
            dma((2, NT - 1)),
            dma((2, 2, 2)),
            dma((2, 5)),
            dma((2, NY)),
            dma((2, 2, 1)),
            dma((2, 2, 2)),
        ],
        compiler_params=pltpu.CompilerParams(
            vmem_limit_bytes=63 * 2**20, collective_id=0, has_side_effects=True
        ),
    )(q, k, vt, w, wd, lambdas, gain, norm_gain, residual, w_out)


def per_device(
    residual, queries, key_pairs, values, lambdas, head_gain, w_out, norm_gain, w_gate, w_up, w_down
):
    return layer(
        queries * jnp.bfloat16(HD**-0.5),
        key_pairs,
        values.T,
        jnp.concatenate([w_gate, w_up], axis=1),
        w_down.T,
        lambdas,
        head_gain[:, None],
        norm_gain[None, :],
        residual,
        w_out,
    )


def solution(mesh):
    torus = Mesh(mesh.devices.reshape(NZ, NX, NT), ("sp_0", "sp_1", "tp"))
    return jax.shard_map(
        per_device,
        mesh=torus,
        in_specs=(
            P(SP, None),
            P(SP, "tp"),
            P(SP, "tp"),
            P(SP, "tp"),
            P("tp"),
            P(),
            P(),
            P(),
            P(SP, "tp"),
            P(SP, "tp"),
            P("tp", SP),
        ),
        out_specs=P(SP_TP, None),
        check_vma=False,
    )
```

time: 207 us -> 145 us (0.70)
  blocking collectives: 59.4 us -> 0 us
  Pallas kernels: 104 us -> 136 us
  between operations: 14.1 us -> 0.66 us
  matrix products: 10.3 us -> 0 us
  waiting for transfers between devices: 5.97 us -> 0 us
  starting transfers between devices: 5.09 us -> 0 us
    all_to_all x2 -> x0, blocking collectives: 59.4 us -> none  [the longest x1 29.7 us: gather_directly(): lax.all_to_all(jnp.broadcast_to(shard[None], (length, *shard.shape)), axi...]
    pallas_call x1, Pallas kernels: 104 us -> 136 us  [layer(): pl.pallas_call(layer_kernel, out_shape=jax.ShapeDtypeStruct((own, model),...]
    dot_general x3 -> x0, matrix products: 10.3 us -> none  [the longest x1 3.75 us: per_device(): lax.dot_general(hidden_units, down_t, (((1,), (1,)), ((), ())), preferred...]
    all_to_all x1 -> x0, waiting for transfers between devices: 5.24 us -> none  [per_device(): lax.all_to_all(heads_out, 'tp', split_axis=0, concat_axis=1, tiled=True)]
    all_to_all x1 -> x0, starting transfers between devices: 5.09 us -> none  [per_device(): lax.all_to_all(heads_out, 'tp', split_axis=0, concat_axis=1, tiled=True)]
  transfers between devices with their start and end apart: 2 -> 0, of which waited for: 1 -> 0; matrix products, arithmetic and copies ran while one was open for 6% -> 0% of each run, Pallas kernels for 50% -> 0%
where the time goes in v3:
time: 145 us
  Pallas kernels  136 us (94%)
  local copies, waits for them, and re-layouts  4.71 us (3%)
  other arithmetic  3.28 us (2%)
    pallas_call x1, Pallas kernels, layer(): pl.pallas_call(layer_kernel, out_shape=jax.ShapeDtypeStruct((own, model),...  136 us
    unnamed x2, local copies, waits for them, and re-layouts  3.33 us

profile of v3, /device:TPU:1, one launch (start us, length us, event | category | flops | bytes accessed | tf_op | source)
XLA Modules:
  0.0 144.7 jit_solution(15129554933489067534)
XLA Ops:
  0.7 1.4 copy.13.gain_ref
  2.0 1.6 %broadcast_multiply_fusion.q_ref = bf16[512,128]{1,0:T(8,128)(2,1)} fusion(bf16[512,128]{1,0:T(8,128)(2,1)} %param.12), kind=kLoop, calls=%fused_computation.1 | loop fusion | flops 65536 | bytes 262144 | tf_op jit(solution)/shard_map/mul | solution.py:606
  3.6 1.7 %copy.12 = bf16[512,128]{0,1:T(8,128)(2,1)} copy(bf16[512,128]{1,0:T(8,128)(2,1)} %param.14) | data formatting | bytes 262144 | tf_op args[3]
  5.3 1.7 %pad_maximum_fusion.w_ref = bf16[64,1408]{1,0:T(8,128)(2,1)} fusion(bf16[64,704]{1,0:T(8,128)(2,1)} %param.20, bf16[64,704]{1,0:T(8,128)(2,1)} %param.19), kind=kLoop, calls=%fused_computation | loop fusion | flops 360448 | bytes 360448 | tf_op jit(solution)/shard_map/concatenate | solution.py:609
  7.0 136.0 %shard_map.109 = bf16[64,2048]{1,0:T(8,128)(2,1)} custom-call(bf16[512,128]{1,0:T(8,128)(2,1)} %broadcast_multiply_fusion.q_ref, bf16[512,128]{1,0:T(8,128)(2,1)} %k_ref.1, bf16[128,512]{1,0:T(8,128)(2,1)} %bitcast.4, bf16[64,1408]{1,0:T(8,128)(2,1)} %pad_maximum_fusion.w_ref, bf16[64,704]{1,0:T(8,128)(2,1)} %bitcast.5, f32[1]{0:T(128)S(6)} %copy.15.lam_ref, ...), custom_call_target="tpu_custom_call" | custom-call | tf_op jit(solution)/shard_map/pallas_call | solution.py:542
  143.0 1.7 %copy.16 = bf16[64,2048]{1,0:T(8,128)(2,1)} copy(bf16[64,2048]{1,0:T(8,128)(2,1)} %shard_map.109) | data formatting | bytes 524288

commit v4 on v3

--- a/solution.py
+++ b/solution.py
@@ -24,11 +24,15 @@
     rows = q.shape[0]
     lane = lax.broadcasted_iota(jnp.int32, q.shape, 1)
     zero = jnp.zeros_like(q)
+    q = q * jnp.asarray(HD**-0.5, q.dtype)
     out_ref[pl.ds(at, rows), :] = jnp.where(lane < HD, q, zero)
     out_ref[pl.ds(at + rows, rows), :] = jnp.where(lane >= HD, q, zero)
 
 
-def attend_tile(q2, keys, values_t, high_ref, acc_ref):
+def attend_tile(q2, keys, values, high_ref, acc_ref):
+    one_row = lax.broadcasted_iota(jnp.int32, (EXTRA, keys.shape[0]), 0) == 0
+    ones = jnp.where(one_row, 1.0, 0.0).astype(values.dtype)
+    values_t = jnp.concatenate([values.T, ones], axis=0)
     scores = lax.dot_general(
         keys, q2, (((1,), (1,)), ((), ())), preferred_element_type=jnp.float32
     )
@@ -74,10 +78,9 @@
 
 
 class Gather:
-    def __init__(self, shard, whole, z, x, z_target, x_target, z_sems, one_sems, two_sems):
-        self.shard, self.whole, self.z, self.x = shard, whole, z, x
+    def __init__(self, rows, whole, z, x, z_target, x_target, z_sems, one_sems, two_sems):
+        self.rows, self.whole, self.z, self.x = rows, whole, z, x
         self.x_target, self.one, self.two = x_target, one_sems, two_sems
-        self.rows = shard.shape[0]
         self.ring = Ring(z_target, self.z_block, z_sems.at[0], z_sems.at[1], (4, 4))
 
     def origin(self, index):
@@ -89,7 +92,7 @@
         rows = pl.ds(0, self.rows) if step < 3 else pl.ds(half * way, half)
         origin = lax.rem(self.z + (NZ - step - at if way == 0 else step + at), NZ)
         ref = self.whole(origin, self.x, rows)
-        return (self.shard if step + at == 0 else ref, ref)
+        return (ref, ref)
 
     def along_x(self, src, dst, sems, way, index):
         return pltpu.make_async_remote_copy(
@@ -105,9 +108,7 @@
         step = number - 1 + at
         from_x = lax.rem(self.x + (NX - step if way == 0 else step), NX)
         ref = self.whole(self.origin(index), from_x, pl.ds(0, self.rows))
-        own = number == 1 and at == 0 and index == 0
-        sems = self.one if number == 1 else self.two
-        return self.along_x(self.shard if own else ref, ref, sems, way, index)
+        return self.along_x(ref, ref, self.one if number == 1 else self.two, way, index)
 
     def members(self, k):
         return [0] if k == 0 else [7] if k == 4 else [2 * k - 1, 2 * k]
@@ -115,11 +116,13 @@
     def second_way(self, index):
         return 0 if index in (0, 1, 3, 5) else 1
 
-    def step(self, k):
+    def along_z(self, k):
         if k > 0:
             self.ring.arrived(k - 1)
         if k < 4:
             self.ring.start(k)
+
+    def both_ways(self, k):
         for index in self.members(k):
             for way in (0, 1):
                 self.hop(1, way, index, 0).start()
@@ -143,7 +146,7 @@
 
 
 def layer_kernel(
-    q_ref, k_ref, vt_ref, w_ref, wd_ref, lam_ref, gain_ref, norm_gain_ref, res_ref, wout_ref,
+    q_ref, k_ref, v_ref, wg_ref, wu_ref, wd_ref, lam_ref, gain_ref, norm_gain_ref, res_ref, wout_ref,
     out_ref,
     qb, kb, vb, q2, high, acc, osend, lsend, orecv, lrecv, orelay,
     wall, down, wout, res, heads, th, normed, hidden, units, parts, pb, pr, fs, fr, relay,
@@ -153,12 +156,10 @@
 ):
     z, x, t = lax.axis_index("sp_0"), lax.axis_index("sp_1"), lax.axis_index("tp")
     y, core = t // 2, lax.rem(t, 2)
-    rows = q_ref.shape[0]
-    width = vt_ref.shape[0]
-    half = w_ref.shape[0] // 2
+    rows, width = vb.shape[1:]
+    wide, unit_width = wg_ref.shape
     columns = 2 * rows
     own = rows // NT
-    unit_width = wd_ref.shape[1]
 
     def z_target(way):
         return {"sp_0": lax.rem(z + (1 if way == 0 else NZ - 1), NZ)}
@@ -178,34 +179,30 @@
         return 0 if step == 0 else 2 * step - 1 if way == 0 else 7 if step == 4 else 2 * step
 
     def k_block(way, step, at):
-        src = k_ref if step + at == 0 else kb.at[slot(way, step + at)]
-        return (src, kb.at[slot(way, step + 1)])
+        return (kb.at[slot(way, step + at)], kb.at[slot(way, step + 1)])
 
     def v_block(way, step, at):
-        inside = vb.at[slot(way, step + at), pl.ds(0, width), :]
-        src = vt_ref if step + at == 0 else inside
-        return (src, vb.at[slot(way, step + 1), pl.ds(0, width), :])
+        return (vb.at[slot(way, step + at)], vb.at[slot(way, step + 1)])
 
     def q_block(way, step, at):
         part = pl.ds(0, rows) if step == 0 else pl.ds(way * (rows // 2), rows // 2)
-        place = lambda hops: (2 if way == 0 else 0) if hops == 1 else 1
-        src = q_ref if step + at == 0 else qb.at[place(step + at), part, :]
-        return (src, qb.at[place(step + 1), part, :])
+        place = lambda hops: (NX - hops if way == 0 else hops) % NX
+        return (qb.at[place(step + at), part, :], qb.at[place(step + 1), part, :])
 
     def ax_block(way, step, at):
-        part = pl.ds(0, half) if step == 0 else pl.ds(way * (half // 2), half // 2)
+        part = pl.ds(0, wide) if step == 0 else pl.ds(way * (wide // 2), wide // 2)
         from_x = lax.rem(x + (NX - step - at if way == 0 else step + at), NX)
         ref = wall.at[z, from_x, part, :]
-        return (w_ref.at[pl.ds(0, half)] if step + at == 0 else ref, ref)
+        return (ref, ref)
 
     def az_block(way, step, at):
         xs = pl.ds(0, NX) if step < 3 else pl.ds(0 if way == 0 else NX // 2, NX // 2)
         origin = lax.rem(z + (NZ - step - at if way == 0 else step + at), NZ)
-        ref = wall.at[origin, xs, pl.ds(0, half), :]
+        ref = wall.at[origin, xs, pl.ds(0, wide), :]
         return (ref, ref)
 
     def b_whole(from_z, from_x, part):
-        return wall.at[from_z, from_x, pl.ds(half + part.start, part.size), :]
+        return wall.at[from_z, from_x, pl.ds(wide + part.start, part.size), :]
 
     def c_whole(from_z, from_x, part):
         return down.at[from_z, from_x, part, :]
@@ -223,9 +220,9 @@
     azring = Ring(z_target, az_block, az_sems.at[0], az_sems.at[1], (4, 4))
     oring = Ring(x_target, o_block, or_sems.at[0], or_sems.at[1], (2, 2))
     later = Gather(
-        w_ref.at[pl.ds(half, half)], b_whole, z, x, z_target, x_target, bz_sems, b1_sems, b2_sems
+        wide, b_whole, z, x, z_target, x_target, bz_sems, b1_sems, b2_sems
     )
-    lowest = Gather(wd_ref, c_whole, z, x, z_target, x_target, cz_sems, c1_sems, c2_sems)
+    lowest = Gather(wide, c_whole, z, x, z_target, x_target, cz_sems, c1_sems, c2_sems)
 
     def x_peer(g, src, dst, sems):
         return pltpu.make_async_remote_copy(
@@ -243,42 +240,42 @@
     def l_copy(g):
         return x_peer(g, lsend.at[g - 1], lrecv.at[g - 1], l_sems)
 
+    locals_ = [
+        pltpu.make_async_copy(src, dst, local_sems.at[i])
+        for i, (src, dst) in enumerate(
+            (
+                (q_ref, qb.at[0]),
+                (k_ref, kb.at[0]),
+                (v_ref, vb.at[0]),
+                (wg_ref, wall.at[z, x, pl.ds(0, wide), :]),
+                (wu_ref, wall.at[z, x, pl.ds(wide, wide), :]),
+                (wd_ref, down.at[z, x]),
+                (res_ref.at[pl.ds(pl.multiple_of(t * own, own), own), :], res),
+                (wout_ref, wout),
+            )
+        )
+    ]
+    for copy in locals_:
+        copy.start()
     barrier = pltpu.get_barrier_semaphore()
     greeted = [{"sp_0": lax.rem(z + s, NZ)} for s in (1, NZ - 1)]
     greeted += [{"sp_1": lax.rem(x + s, NX)} for s in range(1, NX)]
     greeted += [{"tp": lax.rem(t + s, NT)} for s in range(1, NT)]
     for device in greeted:
         pl.semaphore_signal(barrier, inc=1, device_id=device, device_id_type=MESH)
+    high[...] = jnp.full_like(high, LOWEST)
+    acc[...] = jnp.zeros_like(acc)
+    for copy in locals_[:6]:
+        copy.wait()
+    spread_queries(qb[0], q2, 0)
     pl.semaphore_wait(barrier, len(greeted))
 
     qring.start(0)
     kring.start(0)
     vring.start(0)
     axring.start(0)
-    later.step(0)
-    locals_ = [
-        pltpu.make_async_copy(src, dst, local_sems.at[i])
-        for i, (src, dst) in enumerate(
-            (
-                (k_ref, kb.at[0]),
-                (vt_ref, vb.at[0, pl.ds(0, width), :]),
-                (w_ref, wall.at[z, x]),
-                (wd_ref, down.at[z, x]),
-                (res_ref.at[pl.ds(pl.multiple_of(t * own, own), own), :], res),
-                (wout_ref, wout),
-            )
-        )
-    ]
-    for copy in locals_:
-        copy.start()
-    one_row = lax.broadcasted_iota(jnp.int32, (EXTRA, rows), 0) == 0
-    for i in range(NZ):
-        vb[i, pl.ds(width, EXTRA), :] = jnp.where(one_row, 1.0, 0.0).astype(vb.dtype)
-    spread_queries(q_ref[...], q2, 0)
-    high[...] = jnp.full_like(high, LOWEST)
-    acc[...] = jnp.zeros_like(acc)
-    for copy in locals_[:4]:
-        copy.wait()
+    later.along_z(0)
+    later.both_ways(0)
 
     def group_tile(g):
         cols = pl.ds(g * columns, columns)
@@ -299,27 +296,30 @@
     group_tile(0)
     qring.arrived(0)
     qring.start(1)
+    for g in (1, 3):
+        spread_queries(qb[g], q2, g * columns)
+        group_tile(g)
     axring.arrived(0)
     axring.start(1)
-    for g in (1, 3):
-        spread_queries(qb[g - 1], q2, g * columns)
-        group_tile(g)
     kv_step(0)
-    later.step(1)
+    later.along_z(1)
+    later.both_ways(1)
     later.forward(0)
     qring.arrived(1)
-    spread_queries(qb[1], q2, 2 * columns)
+    spread_queries(qb[2], q2, 2 * columns)
     group_tile(2)
-    axring.arrived(1)
-    azring.start(0)
 
     events = {
-        2: [lambda: later.step(2), lambda: later.forward(1)],
         3: [lambda: kv_step(1)],
-        4: [lambda: a_step(0), lambda: later.step(3), lambda: later.forward(2)],
-        5: [lambda: kv_step(2)],
-        6: [lambda: later.step(4), lambda: later.forward(3), lambda: a_step(1), lambda: lowest.step(0)],
-        7: [lambda: kv_step(3)],
+        4: [lambda: later.along_z(2), lambda: later.both_ways(2), lambda: later.forward(1)],
+        5: [lambda: kv_step(2), lambda: axring.arrived(1), lambda: azring.start(0)],
+        6: [lambda: lowest.along_z(0)],
+        7: [
+            lambda: kv_step(3),
+            lambda: later.along_z(3),
+            lambda: later.both_ways(3),
+            lambda: later.forward(2),
+        ],
     }
 
     def tile(i, carry):
@@ -346,8 +346,6 @@
         lsend[g - 1] = jnp.broadcast_to(lse, lsend.shape[1:])
 
     stored(2)
-    lowest.step(1)
-    lowest.forward(0)
     stored(1)
     oring.start(0)
     l_copy(2).start()
@@ -357,12 +355,16 @@
     mix, lse = result(0)
     o_copy(3).start()
     l_copy(3).start()
-    later.forward(4)
-    a_step(2)
+    later.along_z(4)
+    later.both_ways(4)
+    lowest.along_z(1)
+    a_step(0)
     oring.arrived(0)
     oring.start(1)
-    lowest.step(2)
-    lowest.forward(1)
+    later.forward(3)
+    lowest.along_z(2)
+    lowest.both_ways(0)
+    lowest.both_ways(1)
     for g in (1, 3):
         o_copy(g).wait_recv()
     for g in range(1, NX):
@@ -377,10 +379,9 @@
     mix = mix / functools.reduce(jnp.add, shares)
     differ = mix[:, :rows] - lam_ref[0] * mix[:, rows:]
     square = jnp.mean(differ * differ, axis=0, keepdims=True)
-    mine = differ * lax.rsqrt(square + 1e-05) * gain_ref[...]
-    heads[...] = mine.T.astype(heads.dtype)
-    lowest.step(3)
-    lowest.forward(2)
+    mine = (differ * lax.rsqrt(square + 1e-05)).T * gain_ref[...]
+    heads[...] = mine.astype(heads.dtype)
+    later.forward(4)
 
     def own_rows(index):
         return pl.ds(pl.multiple_of(index * own, own), own)
@@ -398,9 +399,11 @@
     for d in range(1, NT):
         h_copy(d, lax.rem(t + d, NT), t).start()
     th[t] = heads[own_rows(t), :]
-    lowest.step(4)
-    lowest.forward(3)
-    for copy in locals_[4:]:
+    a_step(1)
+    lowest.along_z(3)
+    lowest.both_ways(2)
+    lowest.forward(0)
+    for copy in locals_[6:]:
         copy.wait()
     for d in range(1, NT):
         h_copy(d, lax.rem(t + d, NT), lax.rem(t + NT - d, NT)).wait_recv()
@@ -434,38 +437,52 @@
 
     yring.start(0)
     p_copy(0, core).start()
-    lowest.forward(4)
+    lowest.along_z(4)
+    lowest.both_ways(3)
+    lowest.both_ways(4)
+    lowest.forward(1)
     yring.arrived(0)
     yring.start(1)
     p_copy(1, core).start()
     p_copy(2, core).start()
+    a_step(2)
+    lowest.forward(2)
     yring.arrived(1)
     p_copy(3, core).start()
     p_copy(4, core).start()
+    lowest.forward(3)
+    lowest.forward(4)
     later.done()
     azring.arrived(3)
     for number in range(len(shared)):
         p_copy(number, 1 - core).wait_recv()
-    sums = jnp.dot(
-        normed[...].reshape(rows, -1),
-        wall[...].reshape(-1, wall.shape[-1]),
+    inputs = normed[...].reshape(rows, -1)
+    gate = jnp.dot(
+        inputs,
+        wall[:, :, :wide].reshape(-1, unit_width),
         preferred_element_type=jnp.float32,
     )
-    gate, up = sums[:, :unit_width], sums[:, unit_width:]
+    up = jnp.dot(
+        inputs,
+        wall[:, :, wide:].reshape(-1, unit_width),
+        preferred_element_type=jnp.float32,
+    )
     gated = gate / (1.0 + jnp.exp(-gate)) * up
     units[...] = gated.astype(units.dtype).reshape(units.shape)
     lowest.done()
 
-    def piece(offset):
-        lhs = units[pl.ds(chip(offset) * 2, 2)].reshape(2 * own, unit_width)
+    def piece(offsets):
+        lhs = jnp.concatenate([units[pl.ds(chip(o) * 2, 2)] for o in offsets], axis=0)
         part = lax.dot_general(
-            lhs,
+            lhs.reshape(-1, unit_width),
             down[...].reshape(-1, unit_width),
             (((1,), (1,)), ((), ())),
             preferred_element_type=jnp.float32,
         )
-        parts[offset] = part.reshape(parts.shape[1:])
-        pb[offset] = parts[offset, 1 - core].astype(pb.dtype)
+        part = part.reshape(len(offsets), *parts.shape[1:])
+        for i, o in enumerate(offsets):
+            parts[o] = part[i]
+            pb[o] = parts[o, 1 - core].astype(pb.dtype)
 
     def pair_copy(offset):
         return pltpu.make_async_remote_copy(
@@ -492,20 +509,18 @@
 
     rring = Ring(y_target, r_block, r_sems.at[0], r_sems.at[1], (1, 1))
     rrring = Ring(y_target, rr_block, rr_sems.at[0], rr_sems.at[1], (2, 2))
-    piece(2)
-    piece(3)
+    piece((2, 3))
     pair_copy(2).start()
-    piece(1)
     pair_copy(3).start()
+    piece((1, 0))
+    pair_copy(1).start()
+    pair_copy(0).start()
     fs[2] = paired(2).astype(fs.dtype)
-    piece(0)
-    pair_copy(1).start()
+    fs[3] = paired(3).astype(fs.dtype)
     rrring.start(0)
-    fs[3] = paired(3).astype(fs.dtype)
     fs[1] = paired(1).astype(fs.dtype)
-    pair_copy(0).start()
+    total = hidden[...].astype(jnp.float32) + paired(0)
     rring.start(0)
-    total = hidden[...].astype(jnp.float32) + paired(0)
     rrring.arrived(0)
     rrring.start(1)
     rring.arrived(0)
@@ -527,13 +542,12 @@
         pair_copy(offset).wait_send()
 
 
-def layer(q, k, vt, w, wd, lambdas, gain, norm_gain, residual, w_out):
-    rows = q.shape[0]
-    width = vt.shape[0]
+def layer(q, k, v, wg, wu, wd, lambdas, gain, norm_gain, residual, w_out):
+    rows, width = v.shape
     model = residual.shape[1]
     columns = NX * 2 * rows
     own = rows // NT
-    units = wd.shape[1]
+    wide, units = wg.shape
     vmem = pl.BlockSpec(memory_space=pltpu.VMEM)
     smem = pl.BlockSpec(memory_space=pltpu.SMEM)
     hbm = pl.BlockSpec(memory_space=pl.ANY)
@@ -542,12 +556,12 @@
     return pl.pallas_call(
         layer_kernel,
         out_shape=jax.ShapeDtypeStruct((own, model), short),
-        in_specs=[vmem] * 5 + [smem, vmem, vmem, hbm, hbm],
+        in_specs=[hbm] * 6 + [smem, vmem, vmem, hbm, hbm],
         out_specs=vmem,
         scratch_shapes=[
-            pltpu.VMEM((NX - 1, rows, 2 * HD), short),
+            pltpu.VMEM((NX, rows, 2 * HD), short),
             pltpu.VMEM((NZ, rows, 2 * HD), short),
-            pltpu.VMEM((NZ, width + EXTRA, rows), short),
+            pltpu.VMEM((NZ, rows, width), short),
             pltpu.VMEM((columns, 2 * HD), short),
             pltpu.VMEM((1, columns), long),
             pltpu.VMEM((width + EXTRA, columns), long),
@@ -556,7 +570,7 @@
             pltpu.VMEM((NX - 1, width, 2 * rows), short),
             pltpu.VMEM((NX - 1, 8, 2 * rows), long),
             pltpu.VMEM((2, width // 2, 2 * rows), short),
-            pltpu.VMEM((NZ, NX, *w.shape), short),
+            pltpu.VMEM((NZ, NX, 2 * wide, units), short),
             pltpu.VMEM((NZ, NX, *wd.shape), short),
             pltpu.VMEM(w_out.shape, short),
             pltpu.VMEM((own, model), short),
@@ -585,7 +599,7 @@
             dma((2, NX - 1)),
             dma((2, NX - 1)),
             dma((2, 2, 2)),
-            dma((6,)),
+            dma((8,)),
             dma((2, NT - 1)),
             dma((2, 2, 2)),
             dma((2, 5)),
@@ -596,20 +610,21 @@
         compiler_params=pltpu.CompilerParams(
             vmem_limit_bytes=63 * 2**20, collective_id=0, has_side_effects=True
         ),
-    )(q, k, vt, w, wd, lambdas, gain, norm_gain, residual, w_out)
+    )(q, k, v, wg, wu, wd, lambdas, gain, norm_gain, residual, w_out)
 
 
 def per_device(
     residual, queries, key_pairs, values, lambdas, head_gain, w_out, norm_gain, w_gate, w_up, w_down
 ):
     return layer(
-        queries * jnp.bfloat16(HD**-0.5),
+        queries,
         key_pairs,
-        values.T,
-        jnp.concatenate([w_gate, w_up], axis=1),
+        values,
+        w_gate,
+        w_up,
         w_down.T,
         lambdas,
-        head_gain[:, None],
+        head_gain[None, :],
         norm_gain[None, :],
         residual,
         w_out,

time: 145 us -> 115 us (0.79)
  Pallas kernels: 136 us -> 112 us
  other arithmetic: 3.28 us -> 0 us
  local copies, waits for them, and re-layouts: 4.71 us -> 1.67 us
    pallas_call x1, Pallas kernels: 136 us -> 112 us  [layer(): pl.pallas_call(layer_kernel, out_shape=jax.ShapeDtypeStruct((own, model),...]
    concatenate x1 -> x0, other arithmetic: 1.71 us -> none  [per_device(): jnp.concatenate([w_gate, w_up], axis=1)]
    unnamed x2 -> x1, local copies, waits for them, and re-layouts: 3.33 us -> 1.67 us
    mul x1 -> x0, other arithmetic: 1.57 us -> none  [per_device(): queries * jnp.bfloat16(HD ** (-0.5))]
where the time goes in v4:
time: 115 us; the launch traced here: 114 us
  Pallas kernels  112 us (97%)
  local copies, waits for them, and re-layouts  1.67 us (1%)
    pallas_call x1, Pallas kernels, layer(): pl.pallas_call(layer_kernel, out_shape=jax.ShapeDtypeStruct((own, model),...  112 us

profile of v4, /device:TPU:1, one launch (start us, length us, event | category | flops | bytes accessed | tf_op | source)
XLA Modules:
  0.0 114.5 jit_solution(9251707258613856348)
XLA Ops:
  0.7 112.1 %shard_map.109 = bf16[64,2048]{1,0:T(8,128)(2,1)} custom-call(bf16[512,128]{1,0:T(8,128)(2,1)} %q_ref.1, bf16[512,128]{1,0:T(8,128)(2,1)} %k_ref.1, bf16[512,128]{1,0:T(8,128)(2,1)} %v_ref.1, bf16[64,704]{1,0:T(8,128)(2,1)} %wg_ref.1, bf16[64,704]{1,0:T(8,128)(2,1)} %wu_ref.1, bf16[64,704]{1,0:T(8,128)(2,1)} %bitcast.3, f32[1]{0:T(128)S(6)} %copy.13.lam_ref, ...), custom_call_target="tpu_custom_call" | custom-call | tf_op jit(solution)/shard_map/pallas_call | solution.py:556
  112.8 1.7 %copy.14 = bf16[64,2048]{1,0:T(8,128)(2,1)} copy(bf16[64,2048]{1,0:T(8,128)(2,1)} %shard_map.109) | data formatting | bytes 524288

commit v5 on v4

--- a/solution.py
+++ b/solution.py
@@ -13,6 +13,7 @@
 SP_TP = ("sp_0", "sp_1", "tp")
 LOWEST = -1e30
 EXTRA = 16
+SPLIT = 5
 NZ = 8
 NX = 4
 NY = 4
@@ -152,12 +153,13 @@
     wall, down, wout, res, heads, th, normed, hidden, units, parts, pb, pr, fs, fr, relay,
     q_sems, k_sems, v_sems, ax_sems, az_sems, bz_sems, b1_sems, b2_sems,
     cz_sems, c1_sems, c2_sems, o_sems, l_sems, or_sems, local_sems,
-    h_sems, y_sems, p_sems, c_sems, r_sems, rr_sems,
+    h_sems, y_sems, p_sems, c_sems, r_sems, rr_sems, gate_own, up_own,
 ):
     z, x, t = lax.axis_index("sp_0"), lax.axis_index("sp_1"), lax.axis_index("tp")
     y, core = t // 2, lax.rem(t, 2)
     rows, width = vb.shape[1:]
     wide, unit_width = wg_ref.shape
+    half = wide // 2
     columns = 2 * rows
     own = rows // NT
 
@@ -190,7 +192,7 @@
         return (qb.at[place(step + at), part, :], qb.at[place(step + 1), part, :])
 
     def ax_block(way, step, at):
-        part = pl.ds(0, wide) if step == 0 else pl.ds(way * (wide // 2), wide // 2)
+        part = pl.ds(0, half) if step == 0 else pl.ds(way * (half // 2), half // 2)
         from_x = lax.rem(x + (NX - step - at if way == 0 else step + at), NX)
         ref = wall.at[z, from_x, part, :]
         return (ref, ref)
@@ -198,11 +200,11 @@
     def az_block(way, step, at):
         xs = pl.ds(0, NX) if step < 3 else pl.ds(0 if way == 0 else NX // 2, NX // 2)
         origin = lax.rem(z + (NZ - step - at if way == 0 else step + at), NZ)
-        ref = wall.at[origin, xs, pl.ds(0, wide), :]
+        ref = wall.at[origin, xs, pl.ds(0, half), :]
         return (ref, ref)
 
     def b_whole(from_z, from_x, part):
-        return wall.at[from_z, from_x, pl.ds(wide + part.start, part.size), :]
+        return wall.at[from_z, from_x, pl.ds(half + part.start, part.size), :]
 
     def c_whole(from_z, from_x, part):
         return down.at[from_z, from_x, part, :]
@@ -220,7 +222,7 @@
     azring = Ring(z_target, az_block, az_sems.at[0], az_sems.at[1], (4, 4))
     oring = Ring(x_target, o_block, or_sems.at[0], or_sems.at[1], (2, 2))
     later = Gather(
-        wide, b_whole, z, x, z_target, x_target, bz_sems, b1_sems, b2_sems
+        half, b_whole, z, x, z_target, x_target, bz_sems, b1_sems, b2_sems
     )
     lowest = Gather(wide, c_whole, z, x, z_target, x_target, cz_sems, c1_sems, c2_sems)
 
@@ -247,8 +249,8 @@
                 (q_ref, qb.at[0]),
                 (k_ref, kb.at[0]),
                 (v_ref, vb.at[0]),
-                (wg_ref, wall.at[z, x, pl.ds(0, wide), :]),
-                (wu_ref, wall.at[z, x, pl.ds(wide, wide), :]),
+                (wg_ref, gate_own),
+                (wu_ref, up_own),
                 (wd_ref, down.at[z, x]),
                 (res_ref.at[pl.ds(pl.multiple_of(t * own, own), own), :], res),
                 (wout_ref, wout),
@@ -267,6 +269,7 @@
     acc[...] = jnp.zeros_like(acc)
     for copy in locals_[:6]:
         copy.wait()
+    wall[z, x] = jnp.concatenate([gate_own[...], up_own[...]], axis=1)
     spread_queries(qb[0], q2, 0)
     pl.semaphore_wait(barrier, len(greeted))
 
@@ -275,7 +278,6 @@
     vring.start(0)
     axring.start(0)
     later.along_z(0)
-    later.both_ways(0)
 
     def group_tile(g):
         cols = pl.ds(g * columns, columns)
@@ -296,30 +298,26 @@
     group_tile(0)
     qring.arrived(0)
     qring.start(1)
+    later.both_ways(0)
+    kv_step(0)
+    axring.arrived(0)
+    axring.start(1)
     for g in (1, 3):
         spread_queries(qb[g], q2, g * columns)
         group_tile(g)
-    axring.arrived(0)
-    axring.start(1)
-    kv_step(0)
-    later.along_z(1)
-    later.both_ways(1)
-    later.forward(0)
     qring.arrived(1)
     spread_queries(qb[2], q2, 2 * columns)
     group_tile(2)
 
+    def weight_step(gather, k):
+        gather.along_z(k)
+        gather.both_ways(k)
+
     events = {
-        3: [lambda: kv_step(1)],
-        4: [lambda: later.along_z(2), lambda: later.both_ways(2), lambda: later.forward(1)],
-        5: [lambda: kv_step(2), lambda: axring.arrived(1), lambda: azring.start(0)],
-        6: [lambda: lowest.along_z(0)],
-        7: [
-            lambda: kv_step(3),
-            lambda: later.along_z(3),
-            lambda: later.both_ways(3),
-            lambda: later.forward(2),
-        ],
+        1: [lambda: weight_step(later, 1), lambda: later.forward(0)],
+        2: [lambda: kv_step(1)],
+        3: [lambda: weight_step(later, 2), lambda: later.forward(1), lambda: weight_step(lowest, 0)],
+        4: [lambda: kv_step(2), lambda: axring.arrived(1), lambda: azring.start(0)],
     }
 
     def tile(i, carry):
@@ -333,7 +331,13 @@
         attend_tile(q2[...], kb[i], vb[i], high, acc)
         return carry
 
-    lax.fori_loop(1, NZ, tile, 0)
+    lax.fori_loop(1, SPLIT, tile, 0)
+
+    def last_tile(g):
+        cols = pl.ds(g * columns, columns)
+        keys = kb[SPLIT:].reshape(-1, kb.shape[-1])
+        values = vb[SPLIT:].reshape(-1, vb.shape[-1])
+        attend_tile(q2[cols, :], keys, values, high.at[:, cols], acc.at[:, cols])
 
     def result(g):
         cols = pl.ds(g * columns, columns)
@@ -345,26 +349,34 @@
         osend[g - 1] = mix.astype(osend.dtype)
         lsend[g - 1] = jnp.broadcast_to(lse, lsend.shape[1:])
 
+    weight_step(later, 3)
+    later.forward(2)
+    kv_step(3)
+    last_tile(2)
     stored(2)
-    stored(1)
     oring.start(0)
     l_copy(2).start()
-    stored(3)
+    last_tile(1)
+    stored(1)
+    lowest.along_z(1)
     o_copy(1).start()
     l_copy(1).start()
-    mix, lse = result(0)
+    last_tile(3)
+    stored(3)
+    oring.arrived(0)
+    oring.start(1)
     o_copy(3).start()
     l_copy(3).start()
+    lowest.along_z(2)
+    a_step(0)
+    last_tile(0)
+    mix, lse = result(0)
+    lowest.both_ways(1)
     later.along_z(4)
     later.both_ways(4)
-    lowest.along_z(1)
-    a_step(0)
-    oring.arrived(0)
-    oring.start(1)
     later.forward(3)
-    lowest.along_z(2)
-    lowest.both_ways(0)
-    lowest.both_ways(1)
+    lowest.forward(0)
+    lowest.along_z(3)
     for g in (1, 3):
         o_copy(g).wait_recv()
     for g in range(1, NX):
@@ -381,7 +393,6 @@
     square = jnp.mean(differ * differ, axis=0, keepdims=True)
     mine = (differ * lax.rsqrt(square + 1e-05)).T * gain_ref[...]
     heads[...] = mine.astype(heads.dtype)
-    later.forward(4)
 
     def own_rows(index):
         return pl.ds(pl.multiple_of(index * own, own), own)
@@ -400,9 +411,8 @@
         h_copy(d, lax.rem(t + d, NT), t).start()
     th[t] = heads[own_rows(t), :]
     a_step(1)
-    lowest.along_z(3)
     lowest.both_ways(2)
-    lowest.forward(0)
+    lowest.both_ways(3)
     for copy in locals_[6:]:
         copy.wait()
     for d in range(1, NT):
@@ -416,11 +426,12 @@
     normed[t] = (stream * scale * norm_gain_ref[...]).astype(normed.dtype)
 
     def y_block(way, step, at):
-        part = pl.ds(0, own) if step == 0 else pl.ds(way * (own // 2), own // 2)
-        ref = normed.at[chip(NY - step - at if way == 0 else step + at) * 2 + core, part, :]
+        part = pl.ds((1 - way if step == 1 else way) * (own // 2), own // 2)
+        hops = step // 2 + at
+        ref = normed.at[chip(NY - hops if way == 0 else hops) * 2 + core, part, :]
         return (ref, ref)
 
-    yring = Ring(y_target, y_block, y_sems.at[0], y_sems.at[1], (2, 2))
+    yring = Ring(y_target, y_block, y_sems.at[0], y_sems.at[1], (3, 3))
     shared = ((0, 0, own), (NY - 1, 0, own), (1, 0, own), (2, 0, own // 2), (2, own // 2, own // 2))
 
     def p_copy(number, of_core):
@@ -436,37 +447,31 @@
         )
 
     yring.start(0)
+    yring.start(1)
     p_copy(0, core).start()
-    lowest.along_z(4)
-    lowest.both_ways(3)
-    lowest.both_ways(4)
+    weight_step(lowest, 4)
+    later.forward(4)
     lowest.forward(1)
     yring.arrived(0)
-    yring.start(1)
+    yring.start(2)
+    a_step(2)
+    yring.arrived(1)
     p_copy(1, core).start()
     p_copy(2, core).start()
-    a_step(2)
     lowest.forward(2)
-    yring.arrived(1)
+    lowest.forward(3)
+    yring.arrived(2)
     p_copy(3, core).start()
     p_copy(4, core).start()
-    lowest.forward(3)
-    lowest.forward(4)
     later.done()
     azring.arrived(3)
+    lowest.forward(4)
     for number in range(len(shared)):
         p_copy(number, 1 - core).wait_recv()
     inputs = normed[...].reshape(rows, -1)
-    gate = jnp.dot(
-        inputs,
-        wall[:, :, :wide].reshape(-1, unit_width),
-        preferred_element_type=jnp.float32,
-    )
-    up = jnp.dot(
-        inputs,
-        wall[:, :, wide:].reshape(-1, unit_width),
-        preferred_element_type=jnp.float32,
-    )
+    both = wall[...].reshape(-1, wall.shape[-1])
+    sums = jnp.dot(inputs, both, preferred_element_type=jnp.float32)
+    gate, up = sums[:, :unit_width], sums[:, unit_width:]
     gated = gate / (1.0 + jnp.exp(-gate)) * up
     units[...] = gated.astype(units.dtype).reshape(units.shape)
     lowest.done()
@@ -499,16 +504,14 @@
         return parts[offset, core] + pr[offset].astype(jnp.float32)
 
     def r_block(way, step, at):
-        return (fs.at[1 if way == 0 else NY - 1], fr.at[way])
+        part = pl.ds((way if step == 1 else 1 - way) * (own // 2), own // 2)
+        return (fs.at[1 if way == 0 else NY - 1, part, :], fr.at[way, part, :])
 
     def rr_block(way, step, at):
-        part = pl.ds(way * (own // 2), own // 2)
-        if step == 0:
-            return (fs.at[2, part, :], relay.at[way])
-        return (relay.at[way], fr.at[2, part, :])
-
-    rring = Ring(y_target, r_block, r_sems.at[0], r_sems.at[1], (1, 1))
-    rrring = Ring(y_target, rr_block, rr_sems.at[0], rr_sems.at[1], (2, 2))
+        return (fs.at[2, pl.ds(way * (own // 2), own // 2), :], relay.at[way])
+
+    rring = Ring(y_target, r_block, r_sems.at[0], r_sems.at[1], (2, 2))
+    rrring = Ring(y_target, rr_block, rr_sems.at[0], rr_sems.at[1], (1, 1))
     piece((2, 3))
     pair_copy(2).start()
     pair_copy(3).start()
@@ -516,17 +519,21 @@
     pair_copy(1).start()
     pair_copy(0).start()
     fs[2] = paired(2).astype(fs.dtype)
-    fs[3] = paired(3).astype(fs.dtype)
     rrring.start(0)
-    fs[1] = paired(1).astype(fs.dtype)
+    ahead = paired(1)
+    fs[1, own // 2 :] = ahead[own // 2 :].astype(fs.dtype)
+    behind = paired(3)
+    fs[3, : own // 2] = behind[: own // 2].astype(fs.dtype)
+    rring.start(0)
     total = hidden[...].astype(jnp.float32) + paired(0)
-    rring.start(0)
     rrring.arrived(0)
-    rrring.start(1)
+    fs[1, : own // 2] = (ahead[: own // 2] + relay[0].astype(jnp.float32)).astype(fs.dtype)
+    fs[3, own // 2 :] = (behind[own // 2 :] + relay[1].astype(jnp.float32)).astype(fs.dtype)
+    rring.start(1)
     rring.arrived(0)
+    rring.arrived(1)
     total = total + fr[0].astype(jnp.float32) + fr[1].astype(jnp.float32)
-    rrring.arrived(1)
-    out_ref[...] = (total + fr[2].astype(jnp.float32)).astype(out_ref.dtype)
+    out_ref[...] = total.astype(out_ref.dtype)
 
     for ring in (kring, vring, qring, axring, azring, oring, later, lowest, yring, rring, rrring):
         ring.sent()
@@ -570,7 +577,7 @@
             pltpu.VMEM((NX - 1, width, 2 * rows), short),
             pltpu.VMEM((NX - 1, 8, 2 * rows), long),
             pltpu.VMEM((2, width // 2, 2 * rows), short),
-            pltpu.VMEM((NZ, NX, 2 * wide, units), short),
+            pltpu.VMEM((NZ, NX, wide, 2 * units), short),
             pltpu.VMEM((NZ, NX, *wd.shape), short),
             pltpu.VMEM(w_out.shape, short),
             pltpu.VMEM((own, model), short),
@@ -583,7 +590,7 @@
             pltpu.VMEM((NY, own, model), short),
             pltpu.VMEM((NY, own, model), short),
             pltpu.VMEM((NY, own, model), short),
-            pltpu.VMEM((NY - 1, own, model), short),
+            pltpu.VMEM((2, own, model), short),
             pltpu.VMEM((2, own // 2, model), short),
             dma((2, 2, 2)),
             dma((2, 2, 4)),
@@ -601,11 +608,13 @@
             dma((2, 2, 2)),
             dma((8,)),
             dma((2, NT - 1)),
-            dma((2, 2, 2)),
+            dma((2, 2, 3)),
             dma((2, 5)),
             dma((2, NY)),
+            dma((2, 2, 2)),
             dma((2, 2, 1)),
-            dma((2, 2, 2)),
+            pltpu.VMEM((wide, units), short),
+            pltpu.VMEM((wide, units), short),
         ],
         compiler_params=pltpu.CompilerParams(
             vmem_limit_bytes=63 * 2**20, collective_id=0, has_side_effects=True

time: 115 us -> 106 us (0.922)
  Pallas kernels: 112 us -> 103 us
    pallas_call x1, Pallas kernels: 112 us -> 103 us  [layer(): pl.pallas_call(layer_kernel, out_shape=jax.ShapeDtypeStruct((own, model),...]
where the time goes in v5:
time: 106 us
  Pallas kernels  103 us (97%)
  local copies, waits for them, and re-layouts  1.67 us (2%)
    pallas_call x1, Pallas kernels, layer(): pl.pallas_call(layer_kernel, out_shape=jax.ShapeDtypeStruct((own, model),...  103 us

profile of v5, /device:TPU:1, one launch (start us, length us, event | category | flops | bytes accessed | tf_op | source)
XLA Modules:
  0.0 105.7 jit_solution(7396588375105144969)
XLA Ops:
  0.7 103.3 %shard_map.109 = bf16[64,2048]{1,0:T(8,128)(2,1)} custom-call(bf16[512,128]{1,0:T(8,128)(2,1)} %q_ref.1, bf16[512,128]{1,0:T(8,128)(2,1)} %k_ref.1, bf16[512,128]{1,0:T(8,128)(2,1)} %v_ref.1, bf16[64,704]{1,0:T(8,128)(2,1)} %wg_ref.1, bf16[64,704]{1,0:T(8,128)(2,1)} %wu_ref.1, bf16[64,704]{1,0:T(8,128)(2,1)} %bitcast.3, f32[1]{0:T(128)S(6)} %copy.13.lam_ref, ...), custom_call_target="tpu_custom_call" | custom-call | tf_op jit(solution)/shard_map/pallas_call | solution.py:563
  104.0 1.7 %copy.14 = bf16[64,2048]{1,0:T(8,128)(2,1)} copy(bf16[64,2048]{1,0:T(8,128)(2,1)} %shard_map.109) | data formatting | bytes 524288

commit v6 on v5

--- a/solution.py
+++ b/solution.py
@@ -154,6 +154,7 @@
     q_sems, k_sems, v_sems, ax_sems, az_sems, bz_sems, b1_sems, b2_sems,
     cz_sems, c1_sems, c2_sems, o_sems, l_sems, or_sems, local_sems,
     h_sems, y_sems, p_sems, c_sems, r_sems, rr_sems, gate_own, up_own,
+    lrelay, lr_sems,
 ):
     z, x, t = lax.axis_index("sp_0"), lax.axis_index("sp_1"), lax.axis_index("tp")
     y, core = t // 2, lax.rem(t, 2)
@@ -209,18 +210,27 @@
     def c_whole(from_z, from_x, part):
         return down.at[from_z, from_x, part, :]
 
+    def o_half(way):
+        return pl.ds(way * (width // 2), width // 2)
+
     def o_block(way, step, at):
-        part = pl.ds(way * (width // 2), width // 2)
-        if step == 0:
-            return (osend.at[1, part, :], orelay.at[way])
-        return (orelay.at[way], orecv.at[1, part, :])
+        return (osend.at[1, o_half(way), :], orelay.at[way])
+
+    def lr_block(way, step, at):
+        return (lsend.at[1], lrelay.at[way])
+
+    def m_block(way, step, at):
+        part = o_half(way if step == 1 else 1 - way)
+        return (osend.at[2 * way, part, :], orecv.at[way, part, :])
 
     kring = Ring(z_target, k_block, k_sems.at[0], k_sems.at[1], (4, 3))
     vring = Ring(z_target, v_block, v_sems.at[0], v_sems.at[1], (3, 4))
     qring = Ring(x_target, q_block, q_sems.at[0], q_sems.at[1], (2, 2))
     axring = Ring(x_target, ax_block, ax_sems.at[0], ax_sems.at[1], (2, 2))
     azring = Ring(z_target, az_block, az_sems.at[0], az_sems.at[1], (4, 4))
-    oring = Ring(x_target, o_block, or_sems.at[0], or_sems.at[1], (2, 2))
+    oring = Ring(x_target, o_block, or_sems.at[0], or_sems.at[1], (1, 1))
+    lring = Ring(x_target, lr_block, lr_sems.at[0], lr_sems.at[1], (1, 1))
+    mring = Ring(x_target, m_block, o_sems.at[0], o_sems.at[1], (2, 2))
     later = Gather(
         half, b_whole, z, x, z_target, x_target, bz_sems, b1_sems, b2_sems
     )
@@ -235,9 +245,6 @@
             device_id={"sp_1": lax.rem(x + g, NX)},
             device_id_type=MESH,
         )
-
-    def o_copy(g):
-        return x_peer(g, osend.at[g - 1], orecv.at[g - 1], o_sems)
 
     def l_copy(g):
         return x_peer(g, lsend.at[g - 1], lrecv.at[g - 1], l_sems)
@@ -352,43 +359,65 @@
     weight_step(later, 3)
     later.forward(2)
     kv_step(3)
+    def joined(way):
+        g = 1 if way == 0 else 3
+        mix, lse = result(g)
+        first = way * (width // 2)
+        mix = mix[first : first + width // 2]
+        other = lrelay[way][:1]
+        top = jnp.maximum(lse, other)
+        here, there = jnp.exp(lse - top), jnp.exp(other - top)
+        mix = (mix * here + orelay[way].astype(jnp.float32) * there) / (here + there)
+        osend[g - 1, first : first + width // 2] = mix.astype(osend.dtype)
+
     last_tile(2)
     stored(2)
     oring.start(0)
+    lring.start(0)
     l_copy(2).start()
     last_tile(1)
     stored(1)
+    mring.copy(0, 0, 0).start()
+    l_copy(1).start()
     lowest.along_z(1)
-    o_copy(1).start()
-    l_copy(1).start()
     last_tile(3)
     stored(3)
+    mring.copy(1, 0, 0).start()
+    l_copy(3).start()
+    a_step(0)
     oring.arrived(0)
-    oring.start(1)
-    o_copy(3).start()
-    l_copy(3).start()
+    lring.arrived(0)
+    joined(0)
+    joined(1)
+    mring.start(1)
     lowest.along_z(2)
-    a_step(0)
     last_tile(0)
     mix, lse = result(0)
-    lowest.both_ways(1)
     later.along_z(4)
     later.both_ways(4)
     later.forward(3)
+    lowest.both_ways(1)
     lowest.forward(0)
-    lowest.along_z(3)
-    for g in (1, 3):
-        o_copy(g).wait_recv()
+    mring.arrived(0)
+    mring.arrived(1)
     for g in range(1, NX):
         l_copy(g).wait_recv()
-    oring.arrived(1)
     lses = [lse] + [lrecv[g][:1] for g in range(NX - 1)]
     top = functools.reduce(jnp.maximum, lses)
-    shares = [jnp.exp(one - top) for one in lses]
-    mix = mix * shares[0]
-    for g in range(NX - 1):
-        mix = mix + orecv[g].astype(jnp.float32) * shares[g + 1]
-    mix = mix / functools.reduce(jnp.add, shares)
+    mine, left, far, right = [jnp.exp(one - top) for one in lses]
+    from_left, from_right = orecv[0].astype(jnp.float32), orecv[1].astype(jnp.float32)
+    mix = jnp.concatenate(
+        [
+            mix[: width // 2] * mine
+            + from_left[: width // 2] * (left + far)
+            + from_right[: width // 2] * right,
+            mix[width // 2 :] * mine
+            + from_left[width // 2 :] * left
+            + from_right[width // 2 :] * (right + far),
+        ],
+        axis=0,
+    )
+    mix = mix / (mine + left + far + right)
     differ = mix[:, :rows] - lam_ref[0] * mix[:, rows:]
     square = jnp.mean(differ * differ, axis=0, keepdims=True)
     mine = (differ * lax.rsqrt(square + 1e-05)).T * gain_ref[...]
@@ -411,6 +440,8 @@
         h_copy(d, lax.rem(t + d, NT), t).start()
     th[t] = heads[own_rows(t), :]
     a_step(1)
+    lowest.along_z(3)
+    later.forward(4)
     lowest.both_ways(2)
     lowest.both_ways(3)
     for copy in locals_[6:]:
@@ -449,20 +480,19 @@
     yring.start(0)
     yring.start(1)
     p_copy(0, core).start()
-    weight_step(lowest, 4)
-    later.forward(4)
-    lowest.forward(1)
     yring.arrived(0)
     yring.start(2)
     a_step(2)
+    weight_step(lowest, 4)
+    lowest.forward(1)
     yring.arrived(1)
     p_copy(1, core).start()
     p_copy(2, core).start()
     lowest.forward(2)
-    lowest.forward(3)
     yring.arrived(2)
     p_copy(3, core).start()
     p_copy(4, core).start()
+    lowest.forward(3)
     later.done()
     azring.arrived(3)
     lowest.forward(4)
@@ -535,10 +565,8 @@
     total = total + fr[0].astype(jnp.float32) + fr[1].astype(jnp.float32)
     out_ref[...] = total.astype(out_ref.dtype)
 
-    for ring in (kring, vring, qring, axring, azring, oring, later, lowest, yring, rring, rrring):
+    for ring in (kring, vring, qring, axring, azring, oring, lring, mring, later, lowest, yring, rring, rrring):
         ring.sent()
-    for g in (1, 3):
-        o_copy(g).wait_send()
     for g in range(1, NX):
         l_copy(g).wait_send()
     for d in range(1, NT):
@@ -574,7 +602,7 @@
             pltpu.VMEM((width + EXTRA, columns), long),
             pltpu.VMEM((NX - 1, width, 2 * rows), short),
             pltpu.VMEM((NX - 1, 8, 2 * rows), long),
-            pltpu.VMEM((NX - 1, width, 2 * rows), short),
+            pltpu.VMEM((2, width, 2 * rows), short),
             pltpu.VMEM((NX - 1, 8, 2 * rows), long),
             pltpu.VMEM((2, width // 2, 2 * rows), short),
             pltpu.VMEM((NZ, NX, wide, 2 * units), short),
@@ -603,9 +631,9 @@
             dma((2, 2, 4)),
             dma((2, 2, NZ)),
             dma((2, 2, NZ)),
+            dma((2, 2, 2)),
             dma((2, NX - 1)),
-            dma((2, NX - 1)),
-            dma((2, 2, 2)),
+            dma((2, 2, 1)),
             dma((8,)),
             dma((2, NT - 1)),
             dma((2, 2, 3)),
@@ -615,6 +643,8 @@
             dma((2, 2, 1)),
             pltpu.VMEM((wide, units), short),
             pltpu.VMEM((wide, units), short),
+            pltpu.VMEM((2, 8, 2 * rows), long),
+            dma((2, 2, 1)),
         ],
         compiler_params=pltpu.CompilerParams(
             vmem_limit_bytes=63 * 2**20, collective_id=0, has_side_effects=True

time: 106 us -> 103 us (0.972)
  Pallas kernels: 103 us -> 101 us
    pallas_call x1, Pallas kernels: 103 us -> 101 us  [layer(): pl.pallas_call(layer_kernel, out_shape=jax.ShapeDtypeStruct((own, model),...]
where the time goes in v6:
time: 103 us
  Pallas kernels  101 us (98%)
  local copies, waits for them, and re-layouts  1.67 us (2%)
    pallas_call x1, Pallas kernels, layer(): pl.pallas_call(layer_kernel, out_shape=jax.ShapeDtypeStruct((own, model),...  101 us

profile of v6, /device:TPU:1, one launch (start us, length us, event | category | flops | bytes accessed | tf_op | source)
XLA Modules:
  0.0 103.0 jit_solution(18281326304969125754)
XLA Ops:
  0.7 100.7 %shard_map.109 = bf16[64,2048]{1,0:T(8,128)(2,1)} custom-call(bf16[512,128]{1,0:T(8,128)(2,1)} %q_ref.1, bf16[512,128]{1,0:T(8,128)(2,1)} %k_ref.1, bf16[512,128]{1,0:T(8,128)(2,1)} %v_ref.1, bf16[64,704]{1,0:T(8,128)(2,1)} %wg_ref.1, bf16[64,704]{1,0:T(8,128)(2,1)} %wu_ref.1, bf16[64,704]{1,0:T(8,128)(2,1)} %bitcast.3, f32[1]{0:T(128)S(6)} %copy.13.lam_ref, ...), custom_call_target="tpu_custom_call" | custom-call | tf_op jit(solution)/shard_map/pallas_call | solution.py:591
  101.4 1.7 %copy.14 = bf16[64,2048]{1,0:T(8,128)(2,1)} copy(bf16[64,2048]{1,0:T(8,128)(2,1)} %shard_map.109) | data formatting | bytes 524288

commit v7 on v6

--- a/solution.py
+++ b/solution.py
@@ -307,6 +307,7 @@
     qring.start(1)
     later.both_ways(0)
     kv_step(0)
+    lowest.both_ways(0)
     axring.arrived(0)
     axring.start(1)
     for g in (1, 3):
@@ -323,8 +324,13 @@
     events = {
         1: [lambda: weight_step(later, 1), lambda: later.forward(0)],
         2: [lambda: kv_step(1)],
-        3: [lambda: weight_step(later, 2), lambda: later.forward(1), lambda: weight_step(lowest, 0)],
-        4: [lambda: kv_step(2), lambda: axring.arrived(1), lambda: azring.start(0)],
+        3: [lambda: weight_step(later, 2), lambda: later.forward(1), lambda: lowest.along_z(0)],
+        4: [
+            lambda: kv_step(2),
+            lambda: axring.arrived(1),
+            lambda: azring.start(0),
+            lambda: lowest.forward(0),
+        ],
     }
 
     def tile(i, carry):
@@ -397,7 +403,6 @@
     later.both_ways(4)
     later.forward(3)
     lowest.both_ways(1)
-    lowest.forward(0)
     mring.arrived(0)
     mring.arrived(1)
     for g in range(1, NX):

time: 103 us -> 103 us (level)
  no operation moved by 1% of the time
where the time goes in v7:
time: 103 us
  Pallas kernels  101 us (98%)
  local copies, waits for them, and re-layouts  1.67 us (2%)
    pallas_call x1, Pallas kernels, layer(): pl.pallas_call(layer_kernel, out_shape=jax.ShapeDtypeStruct((own, model),...  101 us

profile of v7, /device:TPU:1, one launch (start us, length us, event | category | flops | bytes accessed | tf_op | source)
XLA Modules:
  0.0 103.0 jit_solution(17920918467632991096)
XLA Ops:
  0.7 100.7 %shard_map.109 = bf16[64,2048]{1,0:T(8,128)(2,1)} custom-call(bf16[512,128]{1,0:T(8,128)(2,1)} %q_ref.1, bf16[512,128]{1,0:T(8,128)(2,1)} %k_ref.1, bf16[512,128]{1,0:T(8,128)(2,1)} %v_ref.1, bf16[64,704]{1,0:T(8,128)(2,1)} %wg_ref.1, bf16[64,704]{1,0:T(8,128)(2,1)} %wu_ref.1, bf16[64,704]{1,0:T(8,128)(2,1)} %bitcast.3, f32[1]{0:T(128)S(6)} %copy.13.lam_ref, ...), custom_call_target="tpu_custom_call" | custom-call | tf_op jit(solution)/shard_map/pallas_call | solution.py:596
  101.4 1.7 %copy.14 = bf16[64,2048]{1,0:T(8,128)(2,1)} copy(bf16[64,2048]{1,0:T(8,128)(2,1)} %shard_map.109) | data formatting | bytes 524288
